TPU v7x, 512 devices: a whole 4x8x8 slice. The times are simulated.
512 devices in a mesh: dp: 4 (over x), kv: 64 (over z, y), tp: 2 (over core).
Axes of the slice: x: 4, y: 8, z: 8, core: 2. Of those that a mesh axis runs over, the one named last changes fastest.
Arguments:
- tokens: bfloat16 [512, 4, 4096], P('dp', None, 'kv'), may hold values from -260 to 260
- norm_gain: bfloat16 [4096], replicated, may hold values from 0.099609375 to 1.8984375
- query_weight: bfloat16 [4096, 2048], P(None, ('tp', 'kv')), may hold values from -0.09375 to 0.09375
- key_weight: bfloat16 [4096, 2048], P(None, ('tp', 'kv')), may hold values from -0.09375 to 0.09375
- value_weight: bfloat16 [4096, 4096], P(None, ('tp', 'kv')), may hold values from -0.09375 to 0.09375
- gate_weight: bfloat16 [4096, 4096], P(None, ('tp', 'kv')), may hold values from -0.09375 to 0.09375
- out_weight: bfloat16 [4096, 4096], P('tp', 'kv'), may hold values from -0.09375 to 0.09375
- decay_rate: float32 [16], P('tp'), may hold values from 0.02 to 1
- prior_state: float32 [512, 16, 128, 256], P(('dp', 'kv'), 'tp'), may hold values from -0.6 to 0.6
- last_keys: bfloat16 [512, 4, 16, 128], P(('dp', 'kv'), None, 'tp'), may hold values from -0.5390625 to 0.5390625
- last_values: bfloat16 [512, 4, 16, 256], P(('dp', 'kv'), None, 'tp'), may hold values from -6 to 6
- accepted: int32 [512], P(('dp', 'kv')), may hold values from 0 to 4
- lengths: int32 [512], P(('dp', 'kv')), may hold values from 16 to 99999
Outputs:
- retained: bfloat16 [512, 4, 4096], P('dp', None, ('kv', 'tp'))
- new_state: float32 [512, 16, 128, 256], P(('dp', 'kv'), 'tp')
- new_keys: bfloat16 [512, 4, 16, 128], P(('dp', 'kv'), None, 'tp')
- new_values: bfloat16 [512, 4, 16, 256], P(('dp', 'kv'), None, 'tp')
Inputs may be any that keep to these rules, and one draw needn't show every extreme that they name: `accepted`: how many of the last step's 4 proposals were taken.
All inputs are finite; a program needn't handle non-finite values.
Results may differ from a plain program's by a relative error of at most 0.012.
Values may be sent and summed in bfloat16 or wider, within the bound.
No kernel may reach another device: no remote copies, remote signals or barrier semaphores. Data moves between devices by JAX's collectives and lax.ppermute only.
A program may use at most 64 MiB of HBM per device.

v0:
```python
import jax
import jax.numpy as jnp
from jax import lax
from jax.experimental import pallas as pl
from jax.experimental.pallas import tpu as pltpu
from jax.sharding import Mesh
from jax.sharding import PartitionSpec as P


KV = ("far_z", "near_z", "y")
TP_KV = ("tp", *KV)
DP_KV = ("dp", *KV)
KV_TP = (*KV, "tp")


epsilon = 1e-06
FLOAT = jnp.float32
HALF = jnp.bfloat16


def moved(value, axis, target):
    size = lax.axis_size(axis)
    return lax.ppermute(value, axis, [(i, target(i) % size) for i in range(size)])


def scattered(blocks, axes):
    return lax.all_to_all(blocks, axes, 0, 0, tiled=True)


def rotate(field_in, positions):
    half_size = field_in.shape[-1] // 2
    frequency = jnp.power(10000.0, -jnp.arange(half_size, dtype=FLOAT) / half_size)
    angles = positions.astype(FLOAT)[:, :, None, None] * frequency
    cosine, sine_part = (jnp.cos(angles), jnp.sin(angles))
    floats = field_in.astype(FLOAT)
    first_half, second = (floats[..., :half_size], floats[..., half_size:])
    return jnp.concatenate(
        [first_half * cosine - second * sine_part, first_half * sine_part + second * cosine],
        axis=-1,
    )


def next_state(prior_state, last_keys, last_values, accepted, log_decay):
    highest = lax.Precision.HIGHEST
    step_ids = jnp.arange(last_keys.shape[1], dtype=jnp.int32)
    taken_mask = step_ids[None, :] < accepted[:, None]
    power_exp = jnp.maximum(accepted[:, None] - 1 - step_ids[None, :], 0).astype(FLOAT)
    weight = jnp.where(
        taken_mask[:, :, None], jnp.exp(log_decay[None, None, :] * power_exp[:, :, None]), 0.0
    )
    carried = jnp.exp(log_decay[None, :] * accepted[:, None].astype(FLOAT))
    weighted_keys = last_keys.astype(FLOAT) * weight[..., None]
    return carried[:, :, None, None] * prior_state + jnp.einsum(
        "sphd,sphe->shde", weighted_keys, last_values.astype(FLOAT), precision=highest
    )


def retain(query_rot, key_rot, value_rows, taken_state, log_decay):
    highest = lax.Precision.HIGHEST
    step_ids = jnp.arange(query_rot.shape[1], dtype=jnp.int32)
    scores = jnp.einsum(
        "sthd,smhd->shtm", query_rot.astype(FLOAT), key_rot.astype(FLOAT), precision=highest
    )
    offset = (step_ids[:, None] - step_ids[None, :]).astype(FLOAT)
    decay_grid = jnp.where(
        offset[None] >= 0.0, jnp.exp(log_decay[:, None, None] * jnp.maximum(offset, 0.0)[None]), 0.0
    )
    inner_sum = jnp.einsum(
        "shtm,smhe->sthe", scores * decay_grid[None], value_rows.astype(FLOAT), precision=highest
    )
    query_decay = jnp.exp(log_decay[None, :] * (step_ids[:, None].astype(FLOAT) + 1.0))
    cross_sum = jnp.einsum(
        "sthd,shde->sthe",
        query_rot.astype(FLOAT) * query_decay[None, :, :, None],
        taken_state,
        precision=highest,
    )
    return inner_sum + cross_sum


def arrange_kernel(place, w_own, w_near, w_pair, w_far, weights):
    core, parity = place[0], place[1]
    key_cols = w_own.shape[0] // 6
    span = 2 * w_own.shape[0]
    for source, same_core, same_row in (
        (w_own, True, True),
        (w_near, True, False),
        (w_pair, False, True),
        (w_far, False, False),
    ):
        head_group = core if same_core else 1 - core
        later = parity if same_row else 1 - parity
        first = 0
        for size in (key_cols, key_cols, 2 * key_cols, 2 * key_cols):
            start = pl.multiple_of(head_group * span + 2 * first + later * size, 16)
            weights[pl.ds(start, size), :] = source[first : first + size, :]
            first += size


def arrange(place, sources):
    cols, width = sources[0].shape
    vmem = pl.BlockSpec(memory_space=pltpu.VMEM)
    return pl.pallas_call(
        arrange_kernel,
        in_specs=[pl.BlockSpec(memory_space=pltpu.SMEM)] + [vmem] * 4,
        out_specs=vmem,
        out_shape=jax.ShapeDtypeStruct((4 * cols, width), HALF),
        name="arrange",
    )(place, *sources)


def project_kernel(rows, gain, weights, out):
    width = rows.shape[0]
    span = weights.shape[0] // 2
    floats = rows[...].astype(FLOAT)
    squares = jnp.sum(floats * floats, axis=0, keepdims=True)
    row_scale = lax.rsqrt(squares / width + epsilon)
    normed = (floats * row_scale * gain[...].astype(FLOAT)).astype(HALF)
    product = jnp.dot(weights[...], normed, preferred_element_type=FLOAT)
    seqs = out.shape[2]
    for head_group in range(2):
        part = product[head_group * span : (head_group + 1) * span].T
        out[:, head_group] = part.reshape(-1, seqs, span).astype(HALF)


def project(rows, gain, weights):
    vmem = pl.BlockSpec(memory_space=pltpu.VMEM)
    return pl.pallas_call(
        project_kernel,
        in_specs=[vmem] * 3,
        out_specs=vmem,
        out_shape=jax.ShapeDtypeStruct((64, 2, 2, weights.shape[0] // 2), HALF),
        name="project",
    )(rows, gain, weights)


def output_kernel(place, rows, *refs):
    blocks, out, weights, product = refs[:-3], refs[-3], refs[-2], refs[-1]
    here, ring = place[0], 4
    cols = blocks[0].shape[0]
    quarter = cols // 2
    for turn, block in zip((0, 1, 3, 2), blocks):
        start = pl.multiple_of(lax.rem(here + ring - turn, ring) * cols, cols)
        weights[pl.ds(start, cols), :] = block[...]
    total = lax.dot_general(
        rows[...], weights[...], (((1,), (1,)), ((), ())), preferred_element_type=FLOAT
    )
    groups, row_count, lanes = product.shape
    for group in range(groups):
        product[group] = total[:, group * lanes : (group + 1) * lanes]
    proposals = 4
    seqs = row_count // proposals
    for group in range(groups):
        parts = [product[group, pl.ds(p, seqs, stride=proposals), :] for p in range(proposals)]
        for block in range(lanes // quarter):
            pieces = [part[:, block * quarter : (block + 1) * quarter] for part in parts]
            joined = jnp.concatenate(pieces, axis=1)
            out[group * (lanes // quarter) + block] = joined.astype(HALF)


def output_product(place, rows, blocks):
    vmem = pl.BlockSpec(memory_space=pltpu.VMEM)
    cols, depth = blocks[0].shape
    quarter = cols // 2
    row_count = rows.shape[0]
    return pl.pallas_call(
        output_kernel,
        in_specs=[pl.BlockSpec(memory_space=pltpu.SMEM)] + [vmem] * (1 + len(blocks)),
        out_specs=vmem,
        out_shape=jax.ShapeDtypeStruct((8, row_count // 4, 4 * quarter), HALF),
        scratch_shapes=[
            pltpu.VMEM((4 * cols, depth), HALF),
            pltpu.VMEM((4 * cols // 128, row_count, 128), FLOAT),
        ],
        name="output",
    )(place, rows, *blocks)


def shards(
    tokens,
    norm_gain,
    query_weight,
    key_weight,
    value_weight,
    gate_weight,
    out_weight,
    decay_rate,
    prior_state,
    last_keys,
    last_values,
    accepted,
    lengths,
):
    owned_seqs, proposals, own_width = tokens.shape
    local_seqs, heads_here, key_size, value_size = prior_state.shape
    width = norm_gain.shape[0]
    core = lax.axis_index("tp")
    y_index = lax.axis_index("y")
    far_index = lax.axis_index("far_z")

    turned = tokens.transpose(1, 2, 0)
    mine = lax.dynamic_slice_in_dim(turned, 2 * core, 2, 0)
    copies = jnp.broadcast_to(mine[None], (32, 2, own_width, owned_seqs))
    copies = copies.reshape(64, own_width, owned_seqs)
    arrived = scattered(copies, KV)

    w_own = jnp.concatenate(
        [query_weight.T, key_weight.T, value_weight.T, gate_weight.T], axis=0
    )
    w_near = moved(w_own, "y", lambda i: i ^ 1)
    w_pair = moved(w_own, "tp", lambda i: i ^ 1)
    w_far = moved(w_near, "tp", lambda i: i ^ 1)

    o_own = out_weight.T
    out_blocks = [o_own] + [
        moved(o_own, "far_z", lambda i, turn=turn: i + turn) for turn in (1, 3, 2)
    ]

    log_decay = -decay_rate
    taken_state = next_state(prior_state, last_keys, last_values, accepted, log_decay)

    place = jnp.stack([core, y_index & 1]).astype(jnp.int32)
    weights = arrange(place, (w_own, w_near, w_pair, w_far))
    gain = jnp.broadcast_to(norm_gain[:, None], (width, owned_seqs))
    columns = project(arrived.reshape(width, owned_seqs), gain, weights)
    span = columns.shape[-1]
    columns = scattered(columns.reshape(128, local_seqs, span), KV_TP)
    pieces = columns.reshape(8, 4, 2, 2, local_seqs, span)

    def role_rows(first, last, size):
        picked = pieces[..., first:last].transpose(4, 3, 2, 0, 1, 5)
        return picked.reshape(local_seqs, proposals, heads_here, size)

    sixth = span // 6
    query_rows = role_rows(0, sixth, key_size)
    key_rows = role_rows(sixth, 2 * sixth, key_size)
    value_rows = role_rows(2 * sixth, 4 * sixth, value_size)
    gate_rows = role_rows(4 * sixth, 6 * sixth, value_size)
    positions = (lengths + accepted)[:, None] + jnp.arange(proposals, dtype=jnp.int32)[None, :]
    query_rot = rotate(query_rows, positions).astype(HALF)
    key_rot = (rotate(key_rows, positions) * key_size ** (-0.5)).astype(HALF)
    heads_out = retain(query_rot, key_rot, value_rows, taken_state, log_decay)
    head_norm = heads_out * lax.rsqrt(
        jnp.mean(heads_out * heads_out, axis=-1, keepdims=True) + epsilon
    )
    gated = (jax.nn.silu(gate_rows.astype(FLOAT)) * head_norm).astype(HALF)
    depth = heads_here * value_size
    gated = gated.reshape(1, local_seqs * proposals, depth)
    gated = jnp.broadcast_to(gated, (16, local_seqs * proposals, depth))
    gathered = scattered(gated, ("near_z", "y"))
    far_place = far_index.reshape(1).astype(jnp.int32)
    partial_out = output_product(
        far_place, gathered.reshape(16 * local_seqs * proposals, depth), out_blocks
    )
    terms = scattered(partial_out, ("far_z", "tp"))
    terms = terms.reshape(4, 2, *terms.shape[1:]).astype(FLOAT)
    retained = (terms[:, 0] + terms[:, 1]).astype(HALF)
    retained = retained.reshape(owned_seqs, proposals, -1)
    return (retained, taken_state, key_rot, value_rows)


def solution(mesh):
    finer = Mesh(
        mesh.devices.reshape(mesh.shape["dp"], 4, 2, 8, mesh.shape["tp"]), ("dp", *KV, "tp")
    )
    return jax.shard_map(
        shards,
        mesh=finer,
        in_specs=(
            P("dp", None, KV),
            P(),
            P(None, TP_KV),
            P(None, TP_KV),
            P(None, TP_KV),
            P(None, TP_KV),
            P("tp", KV),
            P("tp"),
            P(DP_KV, "tp", None, None),
            P(DP_KV, None, "tp", None),
            P(DP_KV, None, "tp", None),
            P(DP_KV),
            P(DP_KV),
        ),
        out_specs=(
            P("dp", None, KV_TP),
            P(DP_KV, "tp", None, None),
            P(DP_KV, None, "tp", None),
            P(DP_KV, None, "tp", None),
        ),
        check_vma=False,
    )
```

profile of v0, /device:TPU:1, one launch (start us, length us, event | category | flops | bytes accessed | tf_op | source)
XLA Modules:
  0.0 143.1 jit_solution(883362444931639077)
XLA Ops:
  0.7 2.1 %pad_maximum_fusion.w_own = bf16[96,4096]{1,0:T(8,128)(2,1)} fusion(bf16[32,4096]{1,0:T(8,128)(2,1)} %bitcast.57, bf16[32,4096]{1,0:T(8,128)(2,1)} %bitcast.58, bf16[16,4096]{1,0:T(8,128)(2,1)} %bitcast.63, bf16[16,4096]{1,0:T(8,128)(2,1)} %bitcast.64), kind=kLoop, calls=%fused_computation.4 | loop fusion | flops 3145728 | bytes 1572864 | tf_op jit(solution)/shard_map/concatenate | solution.py:207
  2.8 4.0 %collective-permute-start = (bf16[96,4096]{1,0:T(8,128)(2,1)}, bf16[96,4096]{1,0:T(8,128)(2,1)}, u32[]{:S(2)}, u32[]{:S(2)}) collective-permute-start(bf16[96,4096]{1,0:T(8,128)(2,1)} %pad_maximum_fusion.w_own), channel_id=1, source_target_pairs={{0,2},{2,0},{4,6},{6,4},{8,10},{10,8},{12,14},{14,12},{1,3},{3,1},... | collective-permute-start | bytes 2359304 | tf_op jit(solution)/shard_map/ppermute | solution.py:23
  6.8 6.6 %collective-permute-start.1 = (bf16[96,4096]{1,0:T(8,128)(2,1)}, bf16[96,4096]{1,0:T(8,128)(2,1)}, u32[]{:S(2)}, u32[]{:S(2)}) collective-permute-start(bf16[96,4096]{1,0:T(8,128)(2,1)} %pad_maximum_fusion.w_own), channel_id=1, source_target_pairs={{0,1},{1,0},{2,3},{3,2},{4,5},{5,4},{6,7},{7,6},{8,9},{9,8},{10,11... | collective-permute-start | bytes 2359304 | tf_op jit(solution)/shard_map/ppermute | solution.py:23
  13.5 1.2 broadcast_in_dim.28
  14.7 11.6 %all-to-all-start = ((bf16[64,64,128]{2,1,0:T(8,128)(2,1)}), bf16[64,64,128]{2,1,0:T(8,128)(2,1)S(1)}, u32[]{:S(2)}, u32[]{:S(2)}) async-start(bf16[64,64,128]{2,1,0:T(8,128)(2,1)} %bitcast.2), calls=%async_computation | async-start | bytes 2097152 | tf_op jit(solution)/shard_map/all_to_all | solution.py:27
  26.5 0.1 multiply_exponential_fusion.1
  26.7 0.1 exponential_select_fusion.1
  26.7 0.1 multiply_cosine_fusion
  26.9 2.2 %collective-permute-start.2 = (bf16[96,4096]{1,0:T(8,128)(2,1)}, bf16[96,4096]{1,0:T(8,128)(2,1)}, u32[]{:S(2)}, u32[]{:S(2)}) collective-permute-start(bf16[96,4096]{1,0:T(8,128)(2,1)} %collective-permute-done.w_near), channel_id=1, source_target_pairs={{0,1},{1,0},{2,3},{3,2},{4,5},{5,4},{6,7},{7,6},{8,9},{9,8},{10,11... | collective-permute-start | bytes 2359304 | tf_op jit(solution)/shard_map/ppermute | solution.py:23
  29.1 0.6 pad_add_fusion.place
  29.7 0.1 exponential_select_fusion
  29.8 0.1 convert_multiply_fusion.1
  29.9 2.8 %multiply_add_fusion = f32[2,8,128,256]{3,2,1,0:T(8,128)S(1)} fusion(f32[2,8,128,256]{3,2,1,0:T(8,128)} %param.21, f32[2,8]{1,0:T(2,128)S(1)} %multiply_exponential_fusion.1, bf16[2,4,8,256]{3,2,1,0:T(8,128)(2,1)S(1)} %copy-done.8, f32[2,4,8,128]{3,2,1,0:T(8,128)S(1)} %convert_multiply_fusion.1), kind=kOutput, calls=%fused_computation | convolution fusion | flops 26214400 | bytes 4259904 | tf_op jit(solution)/shard_map/sphd,sphe->shde/dot_general | solution.py:53
  32.7 4.4 %arrange.1.weights = bf16[384,4096]{1,0:T(8,128)(2,1)} custom-call(s32[2]{0:T(128)} %pad_add_fusion.place, bf16[96,4096]{1,0:T(8,128)(2,1)} %pad_maximum_fusion.w_own, bf16[96,4096]{1,0:T(8,128)(2,1)} %collective-permute-done.w_near, bf16[96,4096]{1,0:T(8,128)(2,1)} %collective-permute-done.1.w_pair, bf16[96,4096]{1,0:T(8,128)(2,1)} %collective-permute-done.2.w_far), custom_call_target="tpu_custom_call" | custom-call | tf_op jit(solution)/shard_map/arrange/pallas_call | solution.py:103
  37.1 18.1 %all-to-all-done = bf16[64,64,128]{2,1,0:T(8,128)(2,1)S(1)} async-done(((bf16[64,64,128]{2,1,0:T(8,128)(2,1)}), bf16[64,64,128]{2,1,0:T(8,128)(2,1)S(1)}, u32[]{:S(2)}, u32[]{:S(2)}) %all-to-all-start) | async-done | bytes 1048608 | tf_op jit(solution)/shard_map/all_to_all | solution.py:27
  55.3 1.6 %broadcast_in_dim.29.gain = bf16[4096,128]{1,0:T(8,128)(2,1)} broadcast(bf16[4096]{0:T(1024)(128)(2,1)S(1)} %copy-done.11), dimensions={0} | broadcast | bytes 1056768 | tf_op jit(solution)/shard_map/broadcast_in_dim | solution.py:224
  56.9 4.9 %project.1 = bf16[64,2,2,192]{3,2,1,0:T(2,128)(2,1)} custom-call(bf16[4096,128]{1,0:T(8,128)(2,1)} %bitcast.51, bf16[4096,128]{1,0:T(8,128)(2,1)} %broadcast_in_dim.29.gain, bf16[384,4096]{1,0:T(8,128)(2,1)} %arrange.1.weights), custom_call_target="tpu_custom_call" | custom-call | tf_op jit(solution)/shard_map/project/pallas_call | solution.py:128
  61.8 12.0 %all-to-all-start.1 = ((bf16[128,2,192]{2,1,0:T(2,128)(2,1)}), bf16[128,2,192]{2,1,0:T(2,128)(2,1)S(1)}, u32[]{:S(2)}, u32[]{:S(2)}) async-start(bf16[128,2,192]{2,1,0:T(2,128)(2,1)} %bitcast.55), calls=%async_computation.1 | async-start | bytes 262144 | tf_op jit(solution)/shard_map/all_to_all | solution.py:27
  73.8 0.1 multiply_exponential_fusion
  73.9 12.7 %all-to-all-done.1 = bf16[128,2,192]{2,1,0:T(2,128)(2,1)S(1)} async-done(((bf16[128,2,192]{2,1,0:T(2,128)(2,1)}), bf16[128,2,192]{2,1,0:T(2,128)(2,1)S(1)}, u32[]{:S(2)}, u32[]{:S(2)}) %all-to-all-start.1) | async-done | bytes 98336 | tf_op jit(solution)/shard_map/all_to_all | solution.py:27
  86.5 0.1 fusion.12
  86.7 0.1 fusion.11
  86.9 0.1 reshape.247
  87.0 0.1 reshape.248
  87.2 0.1 reshape.244
  87.3 0.1 subtract_convert_fusion
  87.4 0.1 fusion.5
  87.5 0.1 convert_multiply_fusion
  87.6 0.1 convolution_multiply_fusion
  87.7 0.2 fusion.13
  87.9 1.3 multiply_reduce_fusion
  89.2 0.1 reshape.246
  89.4 0.1 fusion.4
  89.5 0.8 broadcast_in_dim.35
  90.3 3.6 %all-to-all-start.2 = ((bf16[16,8,2048]{2,1,0:T(8,128)(2,1)}), bf16[16,8,2048]{2,1,0:T(8,128)(2,1)S(1)}, u32[]{:S(2)}, u32[]{:S(2)}) async-start(bf16[16,8,2048]{2,1,0:T(8,128)(2,1)} %broadcast_in_dim.35), calls=%async_computation.2 | async-start | bytes 1048576 | tf_op jit(solution)/shard_map/all_to_all | solution.py:27
  93.9 2.5 %collective-permute-start.3 = (bf16[64,2048]{1,0:T(8,128)(2,1)S(1)}, bf16[64,2048]{1,0:T(8,128)(2,1)S(1)}, u32[]{:S(2)}, u32[]{:S(2)}) collective-permute-start(bf16[64,2048]{1,0:T(8,128)(2,1)S(1)} %bitcast.60), channel_id=1, source_target_pairs={{0,32},{32,64},{64,96},{96,0},{1,33},{33,65},{65,97},{97,1},{2,34}... | collective-permute-start | bytes 786440 | tf_op jit(solution)/shard_map/ppermute | solution.py:23
  96.5 4.8 %collective-permute-start.4 = (bf16[64,2048]{1,0:T(8,128)(2,1)S(1)}, bf16[64,2048]{1,0:T(8,128)(2,1)S(1)}, u32[]{:S(2)}, u32[]{:S(2)}) collective-permute-start(bf16[64,2048]{1,0:T(8,128)(2,1)S(1)} %bitcast.61), channel_id=1, source_target_pairs={{0,96},{32,0},{64,32},{96,64},{1,97},{33,1},{65,33},{97,65},{2,98}... | collective-permute-start | bytes 786440 | tf_op jit(solution)/shard_map/ppermute | solution.py:23
  101.3 3.2 %collective-permute-start.5 = (bf16[64,2048]{1,0:T(8,128)(2,1)S(1)}, bf16[64,2048]{1,0:T(8,128)(2,1)S(1)}, u32[]{:S(2)}, u32[]{:S(2)}) collective-permute-start(bf16[64,2048]{1,0:T(8,128)(2,1)S(1)} %bitcast.62), channel_id=1, source_target_pairs={{0,64},{32,96},{64,0},{96,32},{1,65},{33,97},{65,1},{97,33},{2,66}... | collective-permute-start | bytes 786440 | tf_op jit(solution)/shard_map/ppermute | solution.py:23
  104.5 11.9 %collective-permute-done.3.refs_1_ = bf16[64,2048]{1,0:T(8,128)(2,1)S(1)} collective-permute-done((bf16[64,2048]{1,0:T(8,128)(2,1)S(1)}, bf16[64,2048]{1,0:T(8,128)(2,1)S(1)}, u32[]{:S(2)}, u32[]{:S(2)}) %collective-permute-start.3) | collective-permute-done | bytes 262176 | tf_op jit(solution)/shard_map/ppermute | solution.py:23
  116.4 5.1 %collective-permute-done.5.refs_3_ = bf16[64,2048]{1,0:T(8,128)(2,1)S(1)} collective-permute-done((bf16[64,2048]{1,0:T(8,128)(2,1)S(1)}, bf16[64,2048]{1,0:T(8,128)(2,1)S(1)}, u32[]{:S(2)}, u32[]{:S(2)}) %collective-permute-start.5) | collective-permute-done | bytes 262176 | tf_op jit(solution)/shard_map/ppermute | solution.py:23
  121.5 0.7 copy-done.7
  122.2 0.2 copy-done.3
  122.4 2.7 %output.1 = bf16[8,32,128]{2,1,0:T(8,128)(2,1)} custom-call(s32[1]{0:T(128)} %bitcast.place, bf16[128,2048]{1,0:T(8,128)(2,1)} %bitcast.52, bf16[64,2048]{1,0:T(8,128)(2,1)} %bitcast.59, bf16[64,2048]{1,0:T(8,128)(2,1)} %copy-done.5, bf16[64,2048]{1,0:T(8,128)(2,1)} %copy-done.6, bf16[64,2048]{1,0:T(8,128)(2,1)} %copy-done.7), custom_call_target="tpu_custom_call" | custom-call | tf_op jit(solution)/shard_map/output/pallas_call | solution.py:166
  125.1 9.7 %all-to-all-start.3 = ((bf16[8,32,128]{2,1,0:T(8,128)(2,1)}), bf16[8,32,128]{2,1,0:T(8,128)(2,1)S(1)}, u32[]{:S(2)}, u32[]{:S(2)}) async-start(bf16[8,32,128]{2,1,0:T(8,128)(2,1)} %output.1), calls=%async_computation.3 | async-start | bytes 131072 | tf_op jit(solution)/shard_map/all_to_all | solution.py:27
  134.8 0.6 copy.37
  135.4 6.8 %all-to-all-done.3 = bf16[8,32,128]{2,1,0:T(8,128)(2,1)S(1)} async-done(((bf16[8,32,128]{2,1,0:T(8,128)(2,1)}), bf16[8,32,128]{2,1,0:T(8,128)(2,1)S(1)}, u32[]{:S(2)}, u32[]{:S(2)}) %all-to-all-start.3) | async-done | bytes 65568 | tf_op jit(solution)/shard_map/all_to_all | solution.py:27
  142.3 0.1 convert_element_type.117
  142.4 0.7 copy.36
  (49 shorter events, 0.4 us)
Async XLA Ops:
  0.6 12.8 %copy-start = (bf16[128,4,64]{0,2,1:T(8,128)(2,1)S(1)}, bf16[128,4,64]{0,2,1:T(8,128)(2,1)}, u32[]{:S(2)}) copy-start(bf16[128,4,64]{0,2,1:T(8,128)(2,1)} %param.13) | copy-start | bytes 196612
  0.6 25.7 %copy-start.12 = (s32[2]{0:T(128)S(1)}, s32[2]{0:T(128)}, u32[]{:S(2)}) copy-start(s32[2]{0:T(128)} %param.24) | copy-start | bytes 28
  0.7 25.8 %copy-start.13 = (s32[2]{0:T(128)S(1)}, s32[2]{0:T(128)}, u32[]{:S(2)}) copy-start(s32[2]{0:T(128)} %param.25) | copy-start | bytes 28
  0.7 25.8 %copy-start.14 = (f32[8]{0:T(128)S(1)}, f32[8]{0:T(128)}, u32[]{:S(2)}) copy-start(f32[8]{0:T(128)} %param.20) | copy-start | bytes 100
  0.7 29.1 %copy-start.10 = (bf16[2,4,8,128]{3,2,1,0:T(8,128)(2,1)S(1)}, bf16[2,4,8,128]{3,2,1,0:T(8,128)(2,1)}, u32[]{:S(2)}) copy-start(bf16[2,4,8,128]{3,2,1,0:T(8,128)(2,1)} %param.22) | copy-start | bytes 49156
  0.7 29.2 %copy-start.8 = (bf16[2,4,8,256]{3,2,1,0:T(8,128)(2,1)S(1)}, bf16[2,4,8,256]{3,2,1,0:T(8,128)(2,1)}, u32[]{:S(2)}) copy-start(bf16[2,4,8,256]{3,2,1,0:T(8,128)(2,1)} %param.23) | copy-start | bytes 98308
  2.8 24.1 %collective-permute-start = (bf16[96,4096]{1,0:T(8,128)(2,1)}, bf16[96,4096]{1,0:T(8,128)(2,1)}, u32[]{:S(2)}, u32[]{:S(2)}) collective-permute-start(bf16[96,4096]{1,0:T(8,128)(2,1)} %pad_maximum_fusion.w_own), channel_id=1, source_target_pairs={{0,2},{2,0},{4,6},{6,4},{8,10},{10,8},{12,14},{14,12},{1,3},{3,1},... | collective-permute-start | bytes 2359304 | tf_op jit(solution)/shard_map/ppermute | solution.py:23
  6.8 25.9 %collective-permute-start.1 = (bf16[96,4096]{1,0:T(8,128)(2,1)}, bf16[96,4096]{1,0:T(8,128)(2,1)}, u32[]{:S(2)}, u32[]{:S(2)}) collective-permute-start(bf16[96,4096]{1,0:T(8,128)(2,1)} %pad_maximum_fusion.w_own), channel_id=1, source_target_pairs={{0,1},{1,0},{2,3},{3,2},{4,5},{5,4},{6,7},{7,6},{8,9},{9,8},{10,11... | collective-permute-start | bytes 2359304 | tf_op jit(solution)/shard_map/ppermute | solution.py:23
  14.7 40.5 %all-to-all-start = ((bf16[64,64,128]{2,1,0:T(8,128)(2,1)}), bf16[64,64,128]{2,1,0:T(8,128)(2,1)S(1)}, u32[]{:S(2)}, u32[]{:S(2)}) async-start(bf16[64,64,128]{2,1,0:T(8,128)(2,1)} %bitcast.2), calls=%async_computation | async-start | bytes 2097152 | tf_op jit(solution)/shard_map/all_to_all | solution.py:27
  26.9 5.8 %collective-permute-start.2 = (bf16[96,4096]{1,0:T(8,128)(2,1)}, bf16[96,4096]{1,0:T(8,128)(2,1)}, u32[]{:S(2)}, u32[]{:S(2)}) collective-permute-start(bf16[96,4096]{1,0:T(8,128)(2,1)} %collective-permute-done.w_near), channel_id=1, source_target_pairs={{0,1},{1,0},{2,3},{3,2},{4,5},{5,4},{6,7},{7,6},{8,9},{9,8},{10,11... | collective-permute-start | bytes 2359304 | tf_op jit(solution)/shard_map/ppermute | solution.py:23
  32.7 55.3 %copy-start.1 = (f32[2,8,128,256]{3,2,1,0:T(8,128)}, f32[2,8,128,256]{3,2,1,0:T(8,128)S(1)}, u32[]{:S(2)}) copy-start(f32[2,8,128,256]{3,2,1,0:T(8,128)S(1)} %multiply_add_fusion) | copy-start | bytes 6291460
  32.7 22.6 %copy-start.11 = (bf16[4096]{0:T(1024)(128)(2,1)S(1)}, bf16[4096]{0:T(1024)(128)(2,1)}, u32[]{:S(2)}) copy-start(bf16[4096]{0:T(1024)(128)(2,1)} %param.14) | copy-start | bytes 24580
  55.3 1.6 %copy-start.2 = (bf16[64,64,128]{2,1,0:T(8,128)(2,1)}, bf16[64,64,128]{2,1,0:T(8,128)(2,1)S(1)}, u32[]{:S(2)}) copy-start(bf16[64,64,128]{2,1,0:T(8,128)(2,1)S(1)} %all-to-all-done) | copy-start | bytes 3145732
  61.8 24.7 %all-to-all-start.1 = ((bf16[128,2,192]{2,1,0:T(2,128)(2,1)}), bf16[128,2,192]{2,1,0:T(2,128)(2,1)S(1)}, u32[]{:S(2)}, u32[]{:S(2)}) async-start(bf16[128,2,192]{2,1,0:T(2,128)(2,1)} %bitcast.55), calls=%async_computation.1 | async-start | bytes 262144 | tf_op jit(solution)/shard_map/all_to_all | solution.py:27
  87.5 2.9 %copy-start.9 = (bf16[2,4,8,128]{3,2,1,0:T(8,128)(2,1)}, bf16[2,4,8,128]{3,2,1,0:T(8,128)(2,1)S(1)}, u32[]{:S(2)}) copy-start(bf16[2,4,8,128]{3,2,1,0:T(8,128)(2,1)S(1)} %fusion.5) | copy-start | bytes 49156
  87.9 6.0 %copy-start.4 = (bf16[2048,64]{0,1:T(8,128)(2,1)S(1)}, bf16[2048,64]{0,1:T(8,128)(2,1)}, u32[]{:S(2)}) copy-start(bf16[2048,64]{0,1:T(8,128)(2,1)} %param.19) | copy-start | bytes 786436
  90.3 31.2 %all-to-all-start.2 = ((bf16[16,8,2048]{2,1,0:T(8,128)(2,1)}), bf16[16,8,2048]{2,1,0:T(8,128)(2,1)S(1)}, u32[]{:S(2)}, u32[]{:S(2)}) async-start(bf16[16,8,2048]{2,1,0:T(8,128)(2,1)} %broadcast_in_dim.35), calls=%async_computation.2 | async-start | bytes 1048576 | tf_op jit(solution)/shard_map/all_to_all | solution.py:27
  93.9 22.5 %collective-permute-start.3 = (bf16[64,2048]{1,0:T(8,128)(2,1)S(1)}, bf16[64,2048]{1,0:T(8,128)(2,1)S(1)}, u32[]{:S(2)}, u32[]{:S(2)}) collective-permute-start(bf16[64,2048]{1,0:T(8,128)(2,1)S(1)} %bitcast.60), channel_id=1, source_target_pairs={{0,32},{32,64},{64,96},{96,0},{1,33},{33,65},{65,97},{97,1},{2,34}... | collective-permute-start | bytes 786440 | tf_op jit(solution)/shard_map/ppermute | solution.py:23
  96.5 19.9 %collective-permute-start.4 = (bf16[64,2048]{1,0:T(8,128)(2,1)S(1)}, bf16[64,2048]{1,0:T(8,128)(2,1)S(1)}, u32[]{:S(2)}, u32[]{:S(2)}) collective-permute-start(bf16[64,2048]{1,0:T(8,128)(2,1)S(1)} %bitcast.61), channel_id=1, source_target_pairs={{0,96},{32,0},{64,32},{96,64},{1,97},{33,1},{65,33},{97,65},{2,98}... | collective-permute-start | bytes 786440 | tf_op jit(solution)/shard_map/ppermute | solution.py:23
  101.3 20.2 %collective-permute-start.5 = (bf16[64,2048]{1,0:T(8,128)(2,1)S(1)}, bf16[64,2048]{1,0:T(8,128)(2,1)S(1)}, u32[]{:S(2)}, u32[]{:S(2)}) collective-permute-start(bf16[64,2048]{1,0:T(8,128)(2,1)S(1)} %bitcast.62), channel_id=1, source_target_pairs={{0,64},{32,96},{64,0},{96,32},{1,65},{33,97},{65,1},{97,33},{2,66}... | collective-permute-start | bytes 786440 | tf_op jit(solution)/shard_map/ppermute | solution.py:23
  116.4 5.1 %copy-start.5 = (bf16[64,2048]{1,0:T(8,128)(2,1)}, bf16[64,2048]{1,0:T(8,128)(2,1)S(1)}, u32[]{:S(2)}) copy-start(bf16[64,2048]{1,0:T(8,128)(2,1)S(1)} %collective-permute-done.3.refs_1_) | copy-start | bytes 786436
  116.4 5.1 %copy-start.6 = (bf16[64,2048]{1,0:T(8,128)(2,1)}, bf16[64,2048]{1,0:T(8,128)(2,1)S(1)}, u32[]{:S(2)}) copy-start(bf16[64,2048]{1,0:T(8,128)(2,1)S(1)} %collective-permute-done.4.refs_2_) | copy-start | bytes 786436
  121.5 0.7 copy-start.7
  121.5 0.9 copy-start.3
  125.1 17.2 %all-to-all-start.3 = ((bf16[8,32,128]{2,1,0:T(8,128)(2,1)}), bf16[8,32,128]{2,1,0:T(8,128)(2,1)S(1)}, u32[]{:S(2)}, u32[]{:S(2)}) async-start(bf16[8,32,128]{2,1,0:T(8,128)(2,1)} %output.1), calls=%async_computation.3 | async-start | bytes 131072 | tf_op jit(solution)/shard_map/all_to_all | solution.py:27
where the time goes:
time: 145 us; the launch traced here: 143 us
  starting transfers between devices  60.4 us (42%)
  waiting for transfers between devices  54.6 us (38%)
  Pallas kernels  12 us (8%)
  local copies, waits for them, and re-layouts  6.88 us (5%)
  matrix products  4.42 us (3%)
  other arithmetic  3.85 us (3%)
    all_to_all x4, waiting for transfers between devices, scattered(): return lax.all_to_all(blocks, axes, 0, 0, tiled=True)  37.6 us
    all_to_all x4, starting transfers between devices, scattered(): return lax.all_to_all(blocks, axes, 0, 0, tiled=True)  36.9 us
    ppermute x6, starting transfers between devices, moved(): lax.ppermute(value, axis, [(i, target(i) % size) for i in range(size)])  23.4 us
    ppermute x6, waiting for transfers between devices, moved(): lax.ppermute(value, axis, [(i, target(i) % size) for i in range(size)])  17 us
    pallas_call x1, Pallas kernels, project(): pl.pallas_call(project_kernel, in_specs=[vmem] * 3, out_specs=vmem, out_s...  4.86 us
    pallas_call x1, Pallas kernels, arrange(): pl.pallas_call(arrange_kernel, in_specs=[pl.BlockSpec(memory_space=pltpu....  4.43 us
  transfers between devices with their start and end apart: 10, of which 5 were waited for; matrix products, arithmetic and copies ran while one was open for 4% of the time, Pallas kernels for 3%

commit v1 on v0

--- a/solution.py
+++ b/solution.py
@@ -25,6 +25,10 @@
 
 def scattered(blocks, axes):
     return lax.all_to_all(blocks, axes, 0, 0, tiled=True)
+
+
+def near(value):
+    return pltpu.with_memory_space_constraint(value, pltpu.VMEM)
 
 
 def rotate(field_in, positions):
@@ -78,7 +82,7 @@
     return inner_sum + cross_sum
 
 
-def arrange_kernel(place, w_own, w_near, w_pair, w_far, weights):
+def arrange_kernel(place, gain, w_own, w_near, w_pair, w_far, weights, columns):
     core, parity = place[0], place[1]
     key_cols = w_own.shape[0] // 6
     span = 2 * w_own.shape[0]
@@ -95,27 +99,40 @@
             start = pl.multiple_of(head_group * span + 2 * first + later * size, 16)
             weights[pl.ds(start, size), :] = source[first : first + size, :]
             first += size
-
-
-def arrange(place, sources):
+    side = gain.shape[1]
+    floats = gain[...].astype(FLOAT)
+    for row in range(gain.shape[0]):
+        square = jnp.broadcast_to(floats[row : row + 1], (side, side)).T
+        columns[row * side : (row + 1) * side, :] = square.astype(HALF)
+
+
+def arrange(place, gain, sources):
     cols, width = sources[0].shape
     vmem = pl.BlockSpec(memory_space=pltpu.VMEM)
+    side = gain.shape[1]
     return pl.pallas_call(
         arrange_kernel,
-        in_specs=[pl.BlockSpec(memory_space=pltpu.SMEM)] + [vmem] * 4,
-        out_specs=vmem,
-        out_shape=jax.ShapeDtypeStruct((4 * cols, width), HALF),
+        in_specs=[pl.BlockSpec(memory_space=pltpu.SMEM)] + [vmem] * 5,
+        out_specs=(vmem, vmem),
+        out_shape=(
+            pltpu.HBM((4 * cols, width), HALF),
+            pltpu.VMEM((width, side), HALF),
+        ),
         name="arrange",
-    )(place, *sources)
-
-
-def project_kernel(rows, gain, weights, out):
+        compiler_params=pltpu.CompilerParams(vmem_limit_bytes=16 << 20),
+    )(place, gain, *sources)
+
+
+def project_kernel(rows, gain, far_weights, out, weights, arrival):
+    fetch = pltpu.make_async_copy(far_weights, weights, arrival)
+    fetch.start()
     width = rows.shape[0]
     span = weights.shape[0] // 2
     floats = rows[...].astype(FLOAT)
     squares = jnp.sum(floats * floats, axis=0, keepdims=True)
     row_scale = lax.rsqrt(squares / width + epsilon)
     normed = (floats * row_scale * gain[...].astype(FLOAT)).astype(HALF)
+    fetch.wait()
     product = jnp.dot(weights[...], normed, preferred_element_type=FLOAT)
     seqs = out.shape[2]
     for head_group in range(2):
@@ -127,11 +144,13 @@
     vmem = pl.BlockSpec(memory_space=pltpu.VMEM)
     return pl.pallas_call(
         project_kernel,
-        in_specs=[vmem] * 3,
+        in_specs=[vmem, vmem, pl.BlockSpec(memory_space=pltpu.HBM)],
         out_specs=vmem,
-        out_shape=jax.ShapeDtypeStruct((64, 2, 2, weights.shape[0] // 2), HALF),
+        out_shape=pltpu.VMEM((64, 2, 2, weights.shape[0] // 2), HALF),
+        scratch_shapes=[pltpu.VMEM(weights.shape, HALF), pltpu.SemaphoreType.DMA],
         name="project",
-    )(rows, gain, weights)
+        compiler_params=pltpu.CompilerParams(vmem_limit_bytes=24 << 20),
+    )(near(rows), near(gain), pltpu.with_memory_space_constraint(weights, pltpu.HBM))
 
 
 def output_kernel(place, rows, *refs):
@@ -139,8 +158,9 @@
     here, ring = place[0], 4
     cols = blocks[0].shape[0]
     quarter = cols // 2
-    for turn, block in zip((0, 1, 3, 2), blocks):
-        start = pl.multiple_of(lax.rem(here + ring - turn, ring) * cols, cols)
+    stride = 2 * place[1] - 1
+    for turn, block in zip((0, stride, -stride, 2), blocks):
+        start = pl.multiple_of(lax.rem(here + ring + turn, ring) * cols, cols)
         weights[pl.ds(start, cols), :] = block[...]
     total = lax.dot_general(
         rows[...], weights[...], (((1,), (1,)), ((), ())), preferred_element_type=FLOAT
@@ -167,13 +187,14 @@
         output_kernel,
         in_specs=[pl.BlockSpec(memory_space=pltpu.SMEM)] + [vmem] * (1 + len(blocks)),
         out_specs=vmem,
-        out_shape=jax.ShapeDtypeStruct((8, row_count // 4, 4 * quarter), HALF),
+        out_shape=pltpu.VMEM((8, row_count // 4, 4 * quarter), HALF),
         scratch_shapes=[
             pltpu.VMEM((4 * cols, depth), HALF),
             pltpu.VMEM((4 * cols // 128, row_count, 128), FLOAT),
         ],
         name="output",
-    )(place, rows, *blocks)
+        compiler_params=pltpu.CompilerParams(vmem_limit_bytes=16 << 20),
+    )(place, near(rows), *blocks)
 
 
 def shards(
@@ -207,25 +228,45 @@
     w_own = jnp.concatenate(
         [query_weight.T, key_weight.T, value_weight.T, gate_weight.T], axis=0
     )
-    w_near = moved(w_own, "y", lambda i: i ^ 1)
+    neighbours = [(2 * y, 2 * (y ^ 1)) for y in range(8)]
+    neighbours += [(2 * y + 1, 2 * (y + (1 if y % 2 else 7)) % 16 + 1) for y in range(8)]
+    w_near = lax.ppermute(w_own, ("y", "tp"), neighbours)
     w_pair = moved(w_own, "tp", lambda i: i ^ 1)
     w_far = moved(w_near, "tp", lambda i: i ^ 1)
 
     o_own = out_weight.T
-    out_blocks = [o_own] + [
-        moved(o_own, "far_z", lambda i, turn=turn: i + turn) for turn in (1, 3, 2)
-    ]
+    ahead = [(2 * i, 2 * ((i + 1) % 4)) for i in range(4)]
+    ahead += [(2 * i + 1, 2 * ((i - 1) % 4) + 1) for i in range(4)]
+    behind = [(target, source) for source, target in ahead]
+
+    def turned_by(value, pairs):
+        return lax.ppermute(value, ("far_z", "tp"), pairs)
+
+    turn_a = turned_by(o_own, ahead)
+    turn_b = turned_by(o_own, behind)
+    turn_c = turned_by(turn_a, ahead)
+    out_blocks = [o_own, turn_a, turn_b, turn_c]
 
     log_decay = -decay_rate
     taken_state = next_state(prior_state, last_keys, last_values, accepted, log_decay)
 
     place = jnp.stack([core, y_index & 1]).astype(jnp.int32)
-    weights = arrange(place, (w_own, w_near, w_pair, w_far))
-    gain = jnp.broadcast_to(norm_gain[:, None], (width, owned_seqs))
+    weights, gain = arrange(
+        place, norm_gain.reshape(-1, owned_seqs), (w_own, w_near, w_pair, w_far)
+    )
     columns = project(arrived.reshape(width, owned_seqs), gain, weights)
     span = columns.shape[-1]
     columns = scattered(columns.reshape(128, local_seqs, span), KV_TP)
     pieces = columns.reshape(8, 4, 2, 2, local_seqs, span)
+    lane = jnp.arange(span)
+    unit = span // 12
+    even_part = jnp.where(lane < 4 * unit, (lane // unit) % 2, (lane // (2 * unit)) % 2) == 0
+    odd_source = (jnp.arange(2) == 1)[:, None, None, None]
+    shifted = (core == 1) & (odd_source == even_part)
+    turned_pieces = jnp.where(
+        odd_source, jnp.roll(pieces, 1, axis=1), jnp.roll(pieces, -1, axis=1)
+    )
+    pieces = jnp.where(shifted, turned_pieces, pieces)
 
     def role_rows(first, last, size):
         picked = pieces[..., first:last].transpose(4, 3, 2, 0, 1, 5)
@@ -248,7 +289,7 @@
     gated = gated.reshape(1, local_seqs * proposals, depth)
     gated = jnp.broadcast_to(gated, (16, local_seqs * proposals, depth))
     gathered = scattered(gated, ("near_z", "y"))
-    far_place = far_index.reshape(1).astype(jnp.int32)
+    far_place = jnp.stack([far_index, core]).astype(jnp.int32)
     partial_out = output_product(
         far_place, gathered.reshape(16 * local_seqs * proposals, depth), out_blocks
     )

time: 145 us -> 136 us (0.938)
  waiting for transfers between devices: 54.6 us -> 44.6 us
  Pallas kernels: 12 us -> 8.81 us
  other arithmetic: 3.85 us -> 7.02 us
    ppermute x6 -> x2, waiting for transfers between devices: 17 us -> 0.01 us  [moved(): lax.ppermute(value, axis, [(i, target(i) % size) for i in range(size)])]
    ppermute x6 -> x2, starting transfers between devices: 23.4 us -> 6.95 us  [moved(): lax.ppermute(value, axis, [(i, target(i) % size) for i in range(size)])]
    ppermute x0 -> x4, starting transfers between devices: none -> 15.3 us  [the longest x3 9.42 us: turned_by(): return lax.ppermute(value, ('far_z', 'tp'), pairs)]
    ppermute x0 -> x4, waiting for transfers between devices: none -> 14.5 us  [the longest x3 14.5 us: turned_by(): return lax.ppermute(value, ('far_z', 'tp'), pairs)]
    all_to_all x4, waiting for transfers between devices: 37.6 us -> 30.1 us  [scattered(): return lax.all_to_all(blocks, axes, 0, 0, tiled=True)]
    unnamed x33 -> x43, local copies, waits for them, and re-layouts: 2.29 us -> 4.78 us
    broadcast_in_dim x1 -> x0, local copies, waits for them, and re-layouts: 1.64 us -> none  [shards(): gain = jnp.broadcast_to(norm_gain[:, None], (width, owned_seqs))]
  transfers between devices with their start and end apart: 10 -> 10, of which waited for: 5 -> 6; matrix products, arithmetic and copies ran while one was open for 4% -> 8% of each run, Pallas kernels for 3% -> 2%
where the time goes in v1:
time: 136 us; the launch traced here: 135 us
  starting transfers between devices  60.1 us (44%)
  waiting for transfers between devices  44.6 us (33%)
  Pallas kernels  8.81 us (6%)
  local copies, waits for them, and re-layouts  7.75 us (6%)
  other arithmetic  7.02 us (5%)
  matrix products  5.75 us (4%)
    all_to_all x4, starting transfers between devices, scattered(): return lax.all_to_all(blocks, axes, 0, 0, tiled=True)  37.8 us
    all_to_all x4, waiting for transfers between devices, scattered(): return lax.all_to_all(blocks, axes, 0, 0, tiled=True)  30.1 us
    ppermute x3, waiting for transfers between devices, turned_by(): return lax.ppermute(value, ('far_z', 'tp'), pairs)  14.5 us
    ppermute x3, starting transfers between devices, turned_by(): return lax.ppermute(value, ('far_z', 'tp'), pairs)  9.42 us
    ppermute x2, starting transfers between devices, moved(): lax.ppermute(value, axis, [(i, target(i) % size) for i in range(size)])  6.95 us
    ppermute x1, starting transfers between devices, shards(): w_near = lax.ppermute(w_own, ('y', 'tp'), neighbours)  5.92 us
    unnamed x43, local copies, waits for them, and re-layouts  4.78 us
    dot_general x1, matrix products, next_state(): jnp.einsum('sphd,sphe->shde', weighted_keys, last_values.astype(FLOAT), p...  4.12 us
  transfers between devices with their start and end apart: 10, of which 6 were waited for; matrix products, arithmetic and copies ran while one was open for 8% of the time, Pallas kernels for 2%

profile of v1, /device:TPU:1, one launch (start us, length us, event | category | flops | bytes accessed | tf_op | source)
XLA Modules:
  0.0 135.0 jit_solution(11040364369708963111)
XLA Ops:
  0.7 1.2 pad_maximum_fusion.w_own
  1.9 5.9 %collective-permute-start = (bf16[96,4096]{1,0:T(8,128)(2,1)S(1)}, bf16[96,4096]{1,0:T(8,128)(2,1)S(1)}, u32[]{:S(2)}, u32[]{:S(2)}) collective-permute-start(bf16[96,4096]{1,0:T(8,128)(2,1)S(1)} %pad_maximum_fusion.w_own), channel_id=1, source_target_pairs={{0,2},{2,0},{4,6},{6,4},{8,10},{10,8},{12,14},{14,12},{1,15},{3,5}... | collective-permute-start | bytes 2359304 | tf_op jit(solution)/shard_map/ppermute | solution.py:233
  7.8 4.8 %collective-permute-start.1 = (bf16[96,4096]{1,0:T(8,128)(2,1)S(1)}, bf16[96,4096]{1,0:T(8,128)(2,1)S(1)}, u32[]{:S(2)}, u32[]{:S(2)}) collective-permute-start(bf16[96,4096]{1,0:T(8,128)(2,1)S(1)} %pad_maximum_fusion.w_own), channel_id=1, source_target_pairs={{0,1},{1,0},{2,3},{3,2},{4,5},{5,4},{6,7},{7,6},{8,9},{9,8},{10,11... | collective-permute-start | bytes 2359304 | tf_op jit(solution)/shard_map/ppermute | solution.py:23
  12.6 1.3 broadcast_in_dim.44
  13.9 11.6 %all-to-all-start = ((bf16[64,64,128]{2,1,0:T(8,128)(2,1)}), bf16[64,64,128]{2,1,0:T(8,128)(2,1)S(1)}, u32[]{:S(2)}, u32[]{:S(2)}) async-start(bf16[64,64,128]{2,1,0:T(8,128)(2,1)} %bitcast.62), calls=%async_computation | async-start | bytes 2097152 | tf_op jit(solution)/shard_map/all_to_all | solution.py:27
  25.5 0.5 iota_compare_fusion.2
  26.0 0.5 fusion.15
  26.7 0.6 multiply_exponential_fusion.1
  27.3 0.7 multiply_exponential_fusion
  28.0 0.6 convert_compare_fusion
  28.6 0.6 convert_maximum_fusion
  29.3 0.1 multiply_cosine_fusion
  29.5 2.2 %collective-permute-start.2 = (bf16[96,4096]{1,0:T(8,128)(2,1)S(1)}, bf16[96,4096]{1,0:T(8,128)(2,1)}, u32[]{:S(2)}, u32[]{:S(2)}) collective-permute-start(bf16[96,4096]{1,0:T(8,128)(2,1)S(1)} %collective-permute-done.w_near), channel_id=1, source_target_pairs={{0,1},{1,0},{2,3},{3,2},{4,5},{5,4},{6,7},{7,6},{8,9},{9,8},{10,11... | collective-permute-start | bytes 2359304 | tf_op jit(solution)/shard_map/ppermute | solution.py:23
  31.7 0.8 exponential_select_fusion
  32.6 4.1 %multiply_add_fusion = f32[2,8,128,256]{3,2,1,0:T(8,128)} fusion(f32[2,8,128,256]{3,2,1,0:T(8,128)} %param.21, f32[2,8]{1,0:T(2,128)} %multiply_exponential_fusion.1, bf16[2,4,8,256]{3,2,1,0:T(8,128)(2,1)S(1)} %copy-done.8, f32[2,4,8,128]{3,2,1,0:T(8,128)S(1)} %convert_multiply_fusion.1), kind=kOutput, calls=%fused_computation | convolution fusion | flops 26214400 | bytes 4259904 | tf_op jit(solution)/shard_map/sphd,sphe->shde/dot_general | solution.py:57
  36.7 0.9 copy-done.3
  37.6 1.1 copy-done.2
  38.8 1.1 copy-done.4
  39.9 3.3 %arrange.1 = (bf16[384,4096]{1,0:T(8,128)(2,1)}, bf16[4096,128]{1,0:T(8,128)(2,1)S(1)}) custom-call(s32[2]{0:T(128)S(1)} %pad_add_fusion.1.place, bf16[32,128]{1,0:T(8,128)(2,1)S(1)} %bitcast.61, bf16[96,4096]{1,0:T(8,128)(2,1)S(1)} %pad_maximum_fusion.w_own, bf16[96,4096]{1,0:T(8,128)(2,1)S(1)} %copy-done.2, bf16[96,4096]{1,0:T(8,128)(2,1)S(1)} %copy-done.4, ...), custom_call_target="tpu_custom_call" | custom-call | tf_op jit(solution)/shard_map/arrange/pallas_call | solution.py:113
  43.2 10.6 %all-to-all-done = bf16[64,64,128]{2,1,0:T(8,128)(2,1)S(1)} async-done(((bf16[64,64,128]{2,1,0:T(8,128)(2,1)}), bf16[64,64,128]{2,1,0:T(8,128)(2,1)S(1)}, u32[]{:S(2)}, u32[]{:S(2)}) %all-to-all-start) | async-done | bytes 1048608 | tf_op jit(solution)/shard_map/all_to_all | solution.py:27
  53.8 3.7 %project.1 = bf16[64,2,2,192]{3,2,1,0:T(2,128)(2,1)} custom-call(bf16[4096,128]{1,0:T(8,128)(2,1)S(1)} %bitcast.56, bf16[4096,128]{1,0:T(8,128)(2,1)S(1)} %get-tuple-element.6.gain, bf16[384,4096]{1,0:T(8,128)(2,1)} %get-tuple-element.7.far_weights), custom_call_target="tpu_custom_call" | custom-call | tf_op jit(solution)/shard_map/project/pallas_call | solution.py:145
  57.5 10.0 %all-to-all-start.1 = ((bf16[128,2,192]{2,1,0:T(2,128)(2,1)}), bf16[128,2,192]{2,1,0:T(2,128)(2,1)S(1)}, u32[]{:S(2)}, u32[]{:S(2)}) async-start(bf16[128,2,192]{2,1,0:T(2,128)(2,1)} %bitcast.11), calls=%async_computation.1 | async-start | bytes 262144 | tf_op jit(solution)/shard_map/all_to_all | solution.py:27
  67.6 12.6 %all-to-all-done.1 = bf16[128,2,192]{2,1,0:T(2,128)(2,1)S(1)} async-done(((bf16[128,2,192]{2,1,0:T(2,128)(2,1)}), bf16[128,2,192]{2,1,0:T(2,128)(2,1)S(1)}, u32[]{:S(2)}, u32[]{:S(2)}) %all-to-all-start.1) | async-done | bytes 98336 | tf_op jit(solution)/shard_map/all_to_all | solution.py:27
  80.2 0.1 fusion.16
  80.7 0.4 fusion.1
  81.0 0.1 convert_bitcast_fusion.1
  81.1 0.1 convert_bitcast_fusion.2
  81.2 0.1 reshape.319
  81.4 0.1 reshape.320
  81.5 0.1 reshape.313
  81.9 0.1 convolution_multiply_fusion
  82.1 0.2 fusion.20
  82.3 1.3 multiply_reduce_fusion
  83.6 0.1 reshape.315
  83.8 0.8 broadcast_in_dim.50
  84.7 3.6 %all-to-all-start.2 = ((bf16[16,8,2048]{2,1,0:T(8,128)(2,1)}), bf16[16,8,2048]{2,1,0:T(8,128)(2,1)S(1)}, u32[]{:S(2)}, u32[]{:S(2)}) async-start(bf16[16,8,2048]{2,1,0:T(8,128)(2,1)} %broadcast_in_dim.50), calls=%async_computation.2 | async-start | bytes 1048576 | tf_op jit(solution)/shard_map/all_to_all | solution.py:27
  88.3 2.9 %collective-permute-start.3 = (bf16[64,2048]{1,0:T(8,128)(2,1)S(1)}, bf16[64,2048]{1,0:T(8,128)(2,1)S(1)}, u32[]{:S(2)}, u32[]{:S(2)}) collective-permute-start(bf16[64,2048]{1,0:T(8,128)(2,1)S(1)} %bitcast.58), channel_id=1, source_target_pairs={{0,32},{32,64},{64,96},{96,0},{1,97},{33,1},{65,33},{97,65},{2,34}... | collective-permute-start | bytes 786440 | tf_op jit(solution)/shard_map/ppermute | solution.py:243
  91.1 3.3 %collective-permute-start.4 = (bf16[64,2048]{1,0:T(8,128)(2,1)S(1)}, bf16[64,2048]{1,0:T(8,128)(2,1)S(1)}, u32[]{:S(2)}, u32[]{:S(2)}) collective-permute-start(bf16[64,2048]{1,0:T(8,128)(2,1)S(1)} %bitcast.59), channel_id=1, source_target_pairs={{32,0},{64,32},{96,64},{0,96},{97,1},{1,33},{33,65},{65,97},{34,2}... | collective-permute-start | bytes 786440 | tf_op jit(solution)/shard_map/ppermute | solution.py:243
  94.5 4.8 %collective-permute-done.3.refs_1_ = bf16[64,2048]{1,0:T(8,128)(2,1)S(1)} collective-permute-done((bf16[64,2048]{1,0:T(8,128)(2,1)S(1)}, bf16[64,2048]{1,0:T(8,128)(2,1)S(1)}, u32[]{:S(2)}, u32[]{:S(2)}) %collective-permute-start.3) | collective-permute-done | bytes 262176 | tf_op jit(solution)/shard_map/ppermute | solution.py:243
  99.3 3.2 %collective-permute-start.5 = (bf16[64,2048]{1,0:T(8,128)(2,1)S(1)}, bf16[64,2048]{1,0:T(8,128)(2,1)S(1)}, u32[]{:S(2)}, u32[]{:S(2)}) collective-permute-start(bf16[64,2048]{1,0:T(8,128)(2,1)S(1)} %collective-permute-done.3.refs_1_), channel_id=1, source_target_pairs={{0,32},{32,64},{64,96},{96,0},{1,97},{33,1},{65,33},{97,65},{2,34}... | collective-permute-start | bytes 786440 | tf_op jit(solution)/shard_map/ppermute | solution.py:243
  102.6 8.1 %collective-permute-done.4.refs_2_ = bf16[64,2048]{1,0:T(8,128)(2,1)S(1)} collective-permute-done((bf16[64,2048]{1,0:T(8,128)(2,1)S(1)}, bf16[64,2048]{1,0:T(8,128)(2,1)S(1)}, u32[]{:S(2)}, u32[]{:S(2)}) %collective-permute-start.4) | collective-permute-done | bytes 262176 | tf_op jit(solution)/shard_map/ppermute | solution.py:243
  110.7 1.5 %collective-permute-done.5.refs_3_ = bf16[64,2048]{1,0:T(8,128)(2,1)S(1)} collective-permute-done((bf16[64,2048]{1,0:T(8,128)(2,1)S(1)}, bf16[64,2048]{1,0:T(8,128)(2,1)S(1)}, u32[]{:S(2)}, u32[]{:S(2)}) %collective-permute-start.5) | collective-permute-done | bytes 262176 | tf_op jit(solution)/shard_map/ppermute | solution.py:243
  112.3 1.9 %output.1 = bf16[8,32,128]{2,1,0:T(8,128)(2,1)} custom-call(s32[2]{0:T(128)S(1)} %pad_add_fusion.place, bf16[128,2048]{1,0:T(8,128)(2,1)S(1)} %bitcast.57, bf16[64,2048]{1,0:T(8,128)(2,1)S(1)} %bitcast.60, bf16[64,2048]{1,0:T(8,128)(2,1)S(1)} %collective-permute-done.3.refs_1_, bf16[64,2048]{1,0:T(8,128)(2,1)S(1)} %collective-permute-done.4.refs_2_, ...), custom_call_target="tpu_custom_call" | custom-call | tf_op jit(solution)/shard_map/output/pallas_call | solution.py:186
  114.2 12.5 %all-to-all-start.3 = ((bf16[8,32,128]{2,1,0:T(8,128)(2,1)}), bf16[8,32,128]{2,1,0:T(8,128)(2,1)S(1)}, u32[]{:S(2)}, u32[]{:S(2)}) async-start(bf16[8,32,128]{2,1,0:T(8,128)(2,1)} %output.1), calls=%async_computation.3 | async-start | bytes 131072 | tf_op jit(solution)/shard_map/all_to_all | solution.py:27
  126.7 0.6 copy.43
  127.3 6.9 %all-to-all-done.3 = bf16[8,32,128]{2,1,0:T(8,128)(2,1)S(1)} async-done(((bf16[8,32,128]{2,1,0:T(8,128)(2,1)}), bf16[8,32,128]{2,1,0:T(8,128)(2,1)S(1)}, u32[]{:S(2)}, u32[]{:S(2)}) %all-to-all-start.3) | async-done | bytes 65568 | tf_op jit(solution)/shard_map/all_to_all | solution.py:27
  134.2 0.1 convert_element_type.117
  134.3 0.7 copy.42
  (64 shorter events, 1.3 us)
Async XLA Ops:
  0.6 12.0 %copy-start = (bf16[128,4,64]{0,2,1:T(8,128)(2,1)S(1)}, bf16[128,4,64]{0,2,1:T(8,128)(2,1)}, u32[]{:S(2)}) copy-start(bf16[128,4,64]{0,2,1:T(8,128)(2,1)} %param.13) | copy-start | bytes 196612
  0.6 25.9 %copy-start.14 = (s32[2]{0:T(128)S(1)}, s32[2]{0:T(128)}, u32[]{:S(2)}) copy-start(s32[2]{0:T(128)} %param.24) | copy-start | bytes 28
  0.7 26.0 %copy-start.15 = (s32[2]{0:T(128)S(1)}, s32[2]{0:T(128)}, u32[]{:S(2)}) copy-start(s32[2]{0:T(128)} %param.25) | copy-start | bytes 28
  0.7 26.0 %copy-start.17 = (f32[8]{0:T(128)S(1)}, f32[8]{0:T(128)}, u32[]{:S(2)}) copy-start(f32[8]{0:T(128)} %param.20) | copy-start | bytes 100
  0.7 31.8 %copy-start.10 = (bf16[2,4,8,128]{3,2,1,0:T(8,128)(2,1)S(1)}, bf16[2,4,8,128]{3,2,1,0:T(8,128)(2,1)}, u32[]{:S(2)}) copy-start(bf16[2,4,8,128]{3,2,1,0:T(8,128)(2,1)} %param.22) | copy-start | bytes 49156
  0.7 31.9 %copy-start.8 = (bf16[2,4,8,256]{3,2,1,0:T(8,128)(2,1)S(1)}, bf16[2,4,8,256]{3,2,1,0:T(8,128)(2,1)}, u32[]{:S(2)}) copy-start(bf16[2,4,8,256]{3,2,1,0:T(8,128)(2,1)} %param.23) | copy-start | bytes 98308
  1.9 27.5 %collective-permute-start = (bf16[96,4096]{1,0:T(8,128)(2,1)S(1)}, bf16[96,4096]{1,0:T(8,128)(2,1)S(1)}, u32[]{:S(2)}, u32[]{:S(2)}) collective-permute-start(bf16[96,4096]{1,0:T(8,128)(2,1)S(1)} %pad_maximum_fusion.w_own), channel_id=1, source_target_pairs={{0,2},{2,0},{4,6},{6,4},{8,10},{10,8},{12,14},{14,12},{1,15},{3,5}... | collective-permute-start | bytes 2359304 | tf_op jit(solution)/shard_map/ppermute | solution.py:233
  7.8 28.9 %collective-permute-start.1 = (bf16[96,4096]{1,0:T(8,128)(2,1)S(1)}, bf16[96,4096]{1,0:T(8,128)(2,1)S(1)}, u32[]{:S(2)}, u32[]{:S(2)}) collective-permute-start(bf16[96,4096]{1,0:T(8,128)(2,1)S(1)} %pad_maximum_fusion.w_own), channel_id=1, source_target_pairs={{0,1},{1,0},{2,3},{3,2},{4,5},{5,4},{6,7},{7,6},{8,9},{9,8},{10,11... | collective-permute-start | bytes 2359304 | tf_op jit(solution)/shard_map/ppermute | solution.py:23
  13.9 39.9 %all-to-all-start = ((bf16[64,64,128]{2,1,0:T(8,128)(2,1)}), bf16[64,64,128]{2,1,0:T(8,128)(2,1)S(1)}, u32[]{:S(2)}, u32[]{:S(2)}) async-start(bf16[64,64,128]{2,1,0:T(8,128)(2,1)} %bitcast.62), calls=%async_computation | async-start | bytes 2097152 | tf_op jit(solution)/shard_map/all_to_all | solution.py:27
  26.7 2.6 %copy-start.11 = (f32[8]{0:T(128)}, f32[8]{0:T(128)S(1)}, u32[]{:S(2)}) copy-start(f32[8]{0:T(128)S(1)} %neg.17) | copy-start | bytes 100
  29.4 7.3 %copy-start.1 = (bf16[96,4096]{1,0:T(8,128)(2,1)}, bf16[96,4096]{1,0:T(8,128)(2,1)S(1)}, u32[]{:S(2)}) copy-start(bf16[96,4096]{1,0:T(8,128)(2,1)S(1)} %collective-permute-done.w_near) | copy-start | bytes 2359300
  29.5 8.2 %collective-permute-start.2 = (bf16[96,4096]{1,0:T(8,128)(2,1)S(1)}, bf16[96,4096]{1,0:T(8,128)(2,1)}, u32[]{:S(2)}, u32[]{:S(2)}) collective-permute-start(bf16[96,4096]{1,0:T(8,128)(2,1)S(1)} %collective-permute-done.w_near), channel_id=1, source_target_pairs={{0,1},{1,0},{2,3},{3,2},{4,5},{5,4},{6,7},{7,6},{8,9},{9,8},{10,11... | collective-permute-start | bytes 2359304 | tf_op jit(solution)/shard_map/ppermute | solution.py:23
  32.6 5.0 %copy-start.6 = (bf16[4096]{0:T(1024)(128)(2,1)S(1)}, bf16[4096]{0:T(1024)(128)(2,1)}, u32[]{:S(2)}) copy-start(bf16[4096]{0:T(1024)(128)(2,1)} %param.14) | copy-start | bytes 24580
  36.7 0.9 copy-start.3
  37.6 1.1 copy-start.2
  38.8 1.1 copy-start.4
  53.8 13.7 %copy-start.13 = (pred[2]{0:T(512)(128)(4,1)S(1)}, pred[2]{0:T(512)(128)(4,1)}, u32[]{:S(2)}) copy-start(pred[2]{0:T(512)(128)(4,1)} %iota_compare_fusion.2) | copy-start | bytes 10
  53.8 13.8 %copy-start.16 = (pred[192]{0:T(512)(128)(4,1)S(1)}, pred[192]{0:T(512)(128)(4,1)}, u32[]{:S(2)}) copy-start(pred[192]{0:T(512)(128)(4,1)} %fusion.15) | copy-start | bytes 580
  57.4 24.4 %copy-start.12 = (f32[4,8]{1,0:T(4,128)S(1)}, f32[4,8]{1,0:T(4,128)}, u32[]{:S(2)}) copy-start(f32[4,8]{1,0:T(4,128)} %multiply_exponential_fusion) | copy-start | bytes 388
  57.5 24.8 %copy-start.7 = (f32[2,8,128,256]{3,2,1,0:T(8,128)S(1)}, f32[2,8,128,256]{3,2,1,0:T(8,128)}, u32[]{:S(2)}) copy-start(f32[2,8,128,256]{3,2,1,0:T(8,128)} %multiply_add_fusion) | copy-start | bytes 6291460
  57.5 22.8 %all-to-all-start.1 = ((bf16[128,2,192]{2,1,0:T(2,128)(2,1)}), bf16[128,2,192]{2,1,0:T(2,128)(2,1)S(1)}, u32[]{:S(2)}, u32[]{:S(2)}) async-start(bf16[128,2,192]{2,1,0:T(2,128)(2,1)} %bitcast.11), calls=%async_computation.1 | async-start | bytes 262144 | tf_op jit(solution)/shard_map/all_to_all | solution.py:27
  81.8 2.9 %copy-start.9 = (bf16[2,4,8,128]{3,2,1,0:T(8,128)(2,1)}, bf16[2,4,8,128]{3,2,1,0:T(8,128)(2,1)S(1)}, u32[]{:S(2)}) copy-start(bf16[2,4,8,128]{3,2,1,0:T(8,128)(2,1)S(1)} %fusion.6) | copy-start | bytes 49156
  82.3 6.0 %copy-start.5 = (bf16[2048,64]{0,1:T(8,128)(2,1)S(1)}, bf16[2048,64]{0,1:T(8,128)(2,1)}, u32[]{:S(2)}) copy-start(bf16[2048,64]{0,1:T(8,128)(2,1)} %param.19) | copy-start | bytes 786436
  84.7 27.6 %all-to-all-start.2 = ((bf16[16,8,2048]{2,1,0:T(8,128)(2,1)}), bf16[16,8,2048]{2,1,0:T(8,128)(2,1)S(1)}, u32[]{:S(2)}, u32[]{:S(2)}) async-start(bf16[16,8,2048]{2,1,0:T(8,128)(2,1)} %broadcast_in_dim.50), calls=%async_computation.2 | async-start | bytes 1048576 | tf_op jit(solution)/shard_map/all_to_all | solution.py:27
  88.3 11.0 %collective-permute-start.3 = (bf16[64,2048]{1,0:T(8,128)(2,1)S(1)}, bf16[64,2048]{1,0:T(8,128)(2,1)S(1)}, u32[]{:S(2)}, u32[]{:S(2)}) collective-permute-start(bf16[64,2048]{1,0:T(8,128)(2,1)S(1)} %bitcast.58), channel_id=1, source_target_pairs={{0,32},{32,64},{64,96},{96,0},{1,97},{33,1},{65,33},{97,65},{2,34}... | collective-permute-start | bytes 786440 | tf_op jit(solution)/shard_map/ppermute | solution.py:243
  91.1 19.6 %collective-permute-start.4 = (bf16[64,2048]{1,0:T(8,128)(2,1)S(1)}, bf16[64,2048]{1,0:T(8,128)(2,1)S(1)}, u32[]{:S(2)}, u32[]{:S(2)}) collective-permute-start(bf16[64,2048]{1,0:T(8,128)(2,1)S(1)} %bitcast.59), channel_id=1, source_target_pairs={{32,0},{64,32},{96,64},{0,96},{97,1},{1,33},{33,65},{65,97},{34,2}... | collective-permute-start | bytes 786440 | tf_op jit(solution)/shard_map/ppermute | solution.py:243
  99.3 13.0 %collective-permute-start.5 = (bf16[64,2048]{1,0:T(8,128)(2,1)S(1)}, bf16[64,2048]{1,0:T(8,128)(2,1)S(1)}, u32[]{:S(2)}, u32[]{:S(2)}) collective-permute-start(bf16[64,2048]{1,0:T(8,128)(2,1)S(1)} %collective-permute-done.3.refs_1_), channel_id=1, source_target_pairs={{0,32},{32,64},{64,96},{96,0},{1,97},{33,1},{65,33},{97,65},{2,34}... | collective-permute-start | bytes 786440 | tf_op jit(solution)/shard_map/ppermute | solution.py:243
  114.2 20.0 %all-to-all-start.3 = ((bf16[8,32,128]{2,1,0:T(8,128)(2,1)}), bf16[8,32,128]{2,1,0:T(8,128)(2,1)S(1)}, u32[]{:S(2)}, u32[]{:S(2)}) async-start(bf16[8,32,128]{2,1,0:T(8,128)(2,1)} %output.1), calls=%async_computation.3 | async-start | bytes 131072 | tf_op jit(solution)/shard_map/all_to_all | solution.py:27

commit v2 on v1

--- a/solution.py
+++ b/solution.py
@@ -77,7 +77,7 @@
         "sthd,shde->sthe",
         query_rot.astype(FLOAT) * query_decay[None, :, :, None],
         taken_state,
-        precision=highest,
+        precision=lax.Precision.HIGH,
     )
     return inner_sum + cross_sum
 
@@ -268,8 +268,8 @@
     )
     pieces = jnp.where(shifted, turned_pieces, pieces)
 
-    def role_rows(first, last, size):
-        picked = pieces[..., first:last].transpose(4, 3, 2, 0, 1, 5)
+    def role_rows(first, last, size, source=pieces):
+        picked = source[..., first:last].transpose(4, 3, 2, 0, 1, 5)
         return picked.reshape(local_seqs, proposals, heads_here, size)
 
     sixth = span // 6
@@ -289,15 +289,17 @@
     gated = gated.reshape(1, local_seqs * proposals, depth)
     gated = jnp.broadcast_to(gated, (16, local_seqs * proposals, depth))
     gathered = scattered(gated, ("near_z", "y"))
+    late_pieces, gathered = lax.optimization_barrier((pieces, gathered))
     far_place = jnp.stack([far_index, core]).astype(jnp.int32)
     partial_out = output_product(
         far_place, gathered.reshape(16 * local_seqs * proposals, depth), out_blocks
     )
     terms = scattered(partial_out, ("far_z", "tp"))
+    new_values = role_rows(2 * sixth, 4 * sixth, value_size, late_pieces)
     terms = terms.reshape(4, 2, *terms.shape[1:]).astype(FLOAT)
     retained = (terms[:, 0] + terms[:, 1]).astype(HALF)
     retained = retained.reshape(owned_seqs, proposals, -1)
-    return (retained, taken_state, key_rot, value_rows)
+    return (retained, taken_state, key_rot, new_values)
 
 
 def solution(mesh):

time: 136 us -> 135 us (level)
  waiting for transfers between devices: 44.6 us -> 43.2 us
    unnamed x43 -> x42, local copies, waits for them, and re-layouts: 4.78 us -> 4.16 us
  transfers between devices with their start and end apart: 10 -> 10, of which waited for: 6 -> 7; matrix products, arithmetic and copies ran while one was open for 8% -> 9% of each run, Pallas kernels for 2% -> 2%
where the time goes in v2:
time: 135 us; the launch traced here: 134 us
  starting transfers between devices  60 us (44%)
  waiting for transfers between devices  43.2 us (32%)
  Pallas kernels  8.79 us (7%)
  other arithmetic  8.19 us (6%)
  local copies, waits for them, and re-layouts  7.97 us (6%)
  matrix products  5.15 us (4%)
    all_to_all x4, starting transfers between devices, scattered(): return lax.all_to_all(blocks, axes, 0, 0, tiled=True)  37.7 us
    all_to_all x4, waiting for transfers between devices, scattered(): return lax.all_to_all(blocks, axes, 0, 0, tiled=True)  29.5 us
    ppermute x3, waiting for transfers between devices, turned_by(): return lax.ppermute(value, ('far_z', 'tp'), pairs)  13.7 us
    ppermute x3, starting transfers between devices, turned_by(): return lax.ppermute(value, ('far_z', 'tp'), pairs)  9.42 us
    ppermute x2, starting transfers between devices, moved(): lax.ppermute(value, axis, [(i, target(i) % size) for i in range(size)])  6.95 us
    ppermute x1, starting transfers between devices, shards(): w_near = lax.ppermute(w_own, ('y', 'tp'), neighbours)  5.92 us
    unnamed x42, local copies, waits for them, and re-layouts  4.16 us
    dot_general x1, matrix products, next_state(): jnp.einsum('sphd,sphe->shde', weighted_keys, last_values.astype(FLOAT), p...  4.12 us
  transfers between devices with their start and end apart: 10, of which 7 were waited for; matrix products, arithmetic and copies ran while one was open for 9% of the time, Pallas kernels for 2%

profile of v2, /device:TPU:1, one launch (start us, length us, event | category | flops | bytes accessed | tf_op | source)
XLA Modules:
  0.0 134.4 jit_solution(16881107561953443300)
XLA Ops:
  0.7 1.2 pad_maximum_fusion.w_own
  1.9 5.9 %collective-permute-start = (bf16[96,4096]{1,0:T(8,128)(2,1)S(1)}, bf16[96,4096]{1,0:T(8,128)(2,1)S(1)}, u32[]{:S(2)}, u32[]{:S(2)}) collective-permute-start(bf16[96,4096]{1,0:T(8,128)(2,1)S(1)} %pad_maximum_fusion.w_own), channel_id=1, source_target_pairs={{0,2},{2,0},{4,6},{6,4},{8,10},{10,8},{12,14},{14,12},{1,15},{3,5}... | collective-permute-start | bytes 2359304 | tf_op jit(solution)/shard_map/ppermute | solution.py:233
  7.8 4.8 %collective-permute-start.1 = (bf16[96,4096]{1,0:T(8,128)(2,1)S(1)}, bf16[96,4096]{1,0:T(8,128)(2,1)S(1)}, u32[]{:S(2)}, u32[]{:S(2)}) collective-permute-start(bf16[96,4096]{1,0:T(8,128)(2,1)S(1)} %pad_maximum_fusion.w_own), channel_id=1, source_target_pairs={{0,1},{1,0},{2,3},{3,2},{4,5},{5,4},{6,7},{7,6},{8,9},{9,8},{10,11... | collective-permute-start | bytes 2359304 | tf_op jit(solution)/shard_map/ppermute | solution.py:23
  12.6 1.3 broadcast_in_dim.44
  13.9 11.6 %all-to-all-start = ((bf16[64,64,128]{2,1,0:T(8,128)(2,1)}), bf16[64,64,128]{2,1,0:T(8,128)(2,1)S(1)}, u32[]{:S(2)}, u32[]{:S(2)}) async-start(bf16[64,64,128]{2,1,0:T(8,128)(2,1)} %bitcast.66), calls=%async_computation | async-start | bytes 2097152 | tf_op jit(solution)/shard_map/all_to_all | solution.py:27
  25.5 0.5 iota_compare_fusion.2
  26.0 0.5 fusion.15
  26.6 0.6 multiply_power_fusion
  27.2 0.6 multiply_exponential_fusion.1
  27.9 0.7 multiply_exponential_fusion
  28.5 0.6 convert_compare_fusion
  29.1 0.6 convert_maximum_fusion
  29.8 0.7 multiply_cosine_fusion
  30.6 2.2 %collective-permute-start.2 = (bf16[96,4096]{1,0:T(8,128)(2,1)S(1)}, bf16[96,4096]{1,0:T(8,128)(2,1)}, u32[]{:S(2)}, u32[]{:S(2)}) collective-permute-start(bf16[96,4096]{1,0:T(8,128)(2,1)S(1)} %collective-permute-done.w_near), channel_id=1, source_target_pairs={{0,1},{1,0},{2,3},{3,2},{4,5},{5,4},{6,7},{7,6},{8,9},{9,8},{10,11... | collective-permute-start | bytes 2359304 | tf_op jit(solution)/shard_map/ppermute | solution.py:23
  32.9 0.8 exponential_select_fusion
  33.8 4.1 %multiply_add_fusion = f32[2,8,128,256]{3,2,1,0:T(8,128)} fusion(f32[2,8,128,256]{3,2,1,0:T(8,128)} %param.21, f32[2,8]{1,0:T(2,128)} %multiply_exponential_fusion.1, bf16[2,4,8,256]{3,2,1,0:T(8,128)(2,1)S(1)} %copy-done.8, f32[2,4,8,128]{3,2,1,0:T(8,128)S(1)} %convert_multiply_fusion.1), kind=kOutput, calls=%fused_computation | convolution fusion | flops 26214400 | bytes 4259904 | tf_op jit(solution)/shard_map/sphd,sphe->shde/dot_general | solution.py:57
  37.9 0.9 copy-done.3
  38.8 1.1 copy-done.2
  40.0 1.1 copy-done.4
  41.1 3.3 %arrange.1 = (bf16[384,4096]{1,0:T(8,128)(2,1)}, bf16[4096,128]{1,0:T(8,128)(2,1)S(1)}) custom-call(s32[2]{0:T(128)S(1)} %pad_add_fusion.1.place, bf16[32,128]{1,0:T(8,128)(2,1)S(1)} %bitcast.65, bf16[96,4096]{1,0:T(8,128)(2,1)S(1)} %pad_maximum_fusion.w_own, bf16[96,4096]{1,0:T(8,128)(2,1)S(1)} %copy-done.2, bf16[96,4096]{1,0:T(8,128)(2,1)S(1)} %copy-done.4, ...), custom_call_target="tpu_custom_call" | custom-call | tf_op jit(solution)/shard_map/arrange/pallas_call | solution.py:113
  44.3 9.4 %all-to-all-done = bf16[64,64,128]{2,1,0:T(8,128)(2,1)S(1)} async-done(((bf16[64,64,128]{2,1,0:T(8,128)(2,1)}), bf16[64,64,128]{2,1,0:T(8,128)(2,1)S(1)}, u32[]{:S(2)}, u32[]{:S(2)}) %all-to-all-start) | async-done | bytes 1048608 | tf_op jit(solution)/shard_map/all_to_all | solution.py:27
  53.8 3.6 %project.1 = bf16[64,2,2,192]{3,2,1,0:T(2,128)(2,1)} custom-call(bf16[4096,128]{1,0:T(8,128)(2,1)S(1)} %bitcast.60, bf16[4096,128]{1,0:T(8,128)(2,1)S(1)} %get-tuple-element.8.gain, bf16[384,4096]{1,0:T(8,128)(2,1)} %get-tuple-element.9.far_weights), custom_call_target="tpu_custom_call" | custom-call | tf_op jit(solution)/shard_map/project/pallas_call | solution.py:145
  57.5 10.1 %all-to-all-start.1 = ((bf16[128,2,192]{2,1,0:T(2,128)(2,1)}), bf16[128,2,192]{2,1,0:T(2,128)(2,1)S(1)}, u32[]{:S(2)}, u32[]{:S(2)}) async-start(bf16[128,2,192]{2,1,0:T(2,128)(2,1)} %bitcast.11), calls=%async_computation.1 | async-start | bytes 262144 | tf_op jit(solution)/shard_map/all_to_all | solution.py:27
  67.6 12.6 %all-to-all-done.1 = bf16[128,2,192]{2,1,0:T(2,128)(2,1)S(1)} async-done(((bf16[128,2,192]{2,1,0:T(2,128)(2,1)}), bf16[128,2,192]{2,1,0:T(2,128)(2,1)S(1)}, u32[]{:S(2)}, u32[]{:S(2)}) %all-to-all-start.1) | async-done | bytes 98336 | tf_op jit(solution)/shard_map/all_to_all | solution.py:27
  80.2 0.1 fusion.16
  80.7 0.4 fusion.1
  81.2 0.1 reshape.323
  81.4 0.1 reshape.324
  81.5 0.1 reshape.316
  81.9 0.1 convolution_multiply_fusion
  82.1 0.2 fusion.20
  82.3 0.7 multiply_reduce_fusion
  83.0 0.1 reshape.319
  83.2 0.8 broadcast_in_dim.50
  84.1 3.6 %all-to-all-start.2 = ((bf16[16,8,2048]{2,1,0:T(8,128)(2,1)}), bf16[16,8,2048]{2,1,0:T(8,128)(2,1)S(1)}, u32[]{:S(2)}, u32[]{:S(2)}) async-start(bf16[16,8,2048]{2,1,0:T(8,128)(2,1)} %broadcast_in_dim.50), calls=%async_computation.2 | async-start | bytes 1048576 | tf_op jit(solution)/shard_map/all_to_all | solution.py:27
  87.7 2.9 %collective-permute-start.3 = (bf16[64,2048]{1,0:T(8,128)(2,1)S(1)}, bf16[64,2048]{1,0:T(8,128)(2,1)S(1)}, u32[]{:S(2)}, u32[]{:S(2)}) collective-permute-start(bf16[64,2048]{1,0:T(8,128)(2,1)S(1)} %bitcast.62), channel_id=1, source_target_pairs={{0,32},{32,64},{64,96},{96,0},{1,97},{33,1},{65,33},{97,65},{2,34}... | collective-permute-start | bytes 786440 | tf_op jit(solution)/shard_map/ppermute | solution.py:243
  90.5 3.3 %collective-permute-start.4 = (bf16[64,2048]{1,0:T(8,128)(2,1)S(1)}, bf16[64,2048]{1,0:T(8,128)(2,1)S(1)}, u32[]{:S(2)}, u32[]{:S(2)}) collective-permute-start(bf16[64,2048]{1,0:T(8,128)(2,1)S(1)} %bitcast.63), channel_id=1, source_target_pairs={{32,0},{64,32},{96,64},{0,96},{97,1},{1,33},{33,65},{65,97},{34,2}... | collective-permute-start | bytes 786440 | tf_op jit(solution)/shard_map/ppermute | solution.py:243
  93.9 4.8 %collective-permute-done.3.refs_1_ = bf16[64,2048]{1,0:T(8,128)(2,1)S(1)} collective-permute-done((bf16[64,2048]{1,0:T(8,128)(2,1)S(1)}, bf16[64,2048]{1,0:T(8,128)(2,1)S(1)}, u32[]{:S(2)}, u32[]{:S(2)}) %collective-permute-start.3) | collective-permute-done | bytes 262176 | tf_op jit(solution)/shard_map/ppermute | solution.py:243
  98.7 3.2 %collective-permute-start.5 = (bf16[64,2048]{1,0:T(8,128)(2,1)S(1)}, bf16[64,2048]{1,0:T(8,128)(2,1)S(1)}, u32[]{:S(2)}, u32[]{:S(2)}) collective-permute-start(bf16[64,2048]{1,0:T(8,128)(2,1)S(1)} %collective-permute-done.3.refs_1_), channel_id=1, source_target_pairs={{0,32},{32,64},{64,96},{96,0},{1,97},{33,1},{65,33},{97,65},{2,34}... | collective-permute-start | bytes 786440 | tf_op jit(solution)/shard_map/ppermute | solution.py:243
  102.0 0.8 all-to-all-done.2
  102.8 7.3 %collective-permute-done.4.refs_2_ = bf16[64,2048]{1,0:T(8,128)(2,1)S(1)} collective-permute-done((bf16[64,2048]{1,0:T(8,128)(2,1)S(1)}, bf16[64,2048]{1,0:T(8,128)(2,1)S(1)}, u32[]{:S(2)}, u32[]{:S(2)}) %collective-permute-start.4) | collective-permute-done | bytes 262176 | tf_op jit(solution)/shard_map/ppermute | solution.py:243
  110.1 1.5 %collective-permute-done.5.refs_3_ = bf16[64,2048]{1,0:T(8,128)(2,1)S(1)} collective-permute-done((bf16[64,2048]{1,0:T(8,128)(2,1)S(1)}, bf16[64,2048]{1,0:T(8,128)(2,1)S(1)}, u32[]{:S(2)}, u32[]{:S(2)}) %collective-permute-start.5) | collective-permute-done | bytes 262176 | tf_op jit(solution)/shard_map/ppermute | solution.py:243
  111.7 1.9 %output.1 = bf16[8,32,128]{2,1,0:T(8,128)(2,1)} custom-call(s32[2]{0:T(128)S(1)} %pad_add_fusion.place, bf16[128,2048]{1,0:T(8,128)(2,1)S(1)} %bitcast.61, bf16[64,2048]{1,0:T(8,128)(2,1)S(1)} %bitcast.64, bf16[64,2048]{1,0:T(8,128)(2,1)S(1)} %collective-permute-done.3.refs_1_, bf16[64,2048]{1,0:T(8,128)(2,1)S(1)} %collective-permute-done.4.refs_2_, ...), custom_call_target="tpu_custom_call" | custom-call | tf_op jit(solution)/shard_map/output/pallas_call | solution.py:186
  113.5 12.5 %all-to-all-start.3 = ((bf16[8,32,128]{2,1,0:T(8,128)(2,1)}), bf16[8,32,128]{2,1,0:T(8,128)(2,1)S(1)}, u32[]{:S(2)}, u32[]{:S(2)}) async-start(bf16[8,32,128]{2,1,0:T(8,128)(2,1)} %output.1), calls=%async_computation.3 | async-start | bytes 131072 | tf_op jit(solution)/shard_map/all_to_all | solution.py:27
  126.1 0.1 reshape.325
  126.2 0.6 copy.48
  126.9 6.7 %all-to-all-done.3 = bf16[8,32,128]{2,1,0:T(8,128)(2,1)S(1)} async-done(((bf16[8,32,128]{2,1,0:T(8,128)(2,1)}), bf16[8,32,128]{2,1,0:T(8,128)(2,1)S(1)}, u32[]{:S(2)}, u32[]{:S(2)}) %all-to-all-start.3) | async-done | bytes 65568 | tf_op jit(solution)/shard_map/all_to_all | solution.py:27
  133.7 0.7 copy.43
  (66 shorter events, 1.7 us)
Async XLA Ops:
  0.6 12.0 %copy-start = (bf16[128,4,64]{0,2,1:T(8,128)(2,1)S(1)}, bf16[128,4,64]{0,2,1:T(8,128)(2,1)}, u32[]{:S(2)}) copy-start(bf16[128,4,64]{0,2,1:T(8,128)(2,1)} %param.13) | copy-start | bytes 196612
  0.6 26.5 %copy-start.14 = (s32[2]{0:T(128)S(1)}, s32[2]{0:T(128)}, u32[]{:S(2)}) copy-start(s32[2]{0:T(128)} %param.24) | copy-start | bytes 28
  0.7 26.5 %copy-start.15 = (s32[2]{0:T(128)S(1)}, s32[2]{0:T(128)}, u32[]{:S(2)}) copy-start(s32[2]{0:T(128)} %param.25) | copy-start | bytes 28
  0.7 26.5 %copy-start.17 = (f32[8]{0:T(128)S(1)}, f32[8]{0:T(128)}, u32[]{:S(2)}) copy-start(f32[8]{0:T(128)} %param.20) | copy-start | bytes 100
  0.7 33.0 %copy-start.10 = (bf16[2,4,8,128]{3,2,1,0:T(8,128)(2,1)S(1)}, bf16[2,4,8,128]{3,2,1,0:T(8,128)(2,1)}, u32[]{:S(2)}) copy-start(bf16[2,4,8,128]{3,2,1,0:T(8,128)(2,1)} %param.22) | copy-start | bytes 49156
  0.7 33.1 %copy-start.8 = (bf16[2,4,8,256]{3,2,1,0:T(8,128)(2,1)S(1)}, bf16[2,4,8,256]{3,2,1,0:T(8,128)(2,1)}, u32[]{:S(2)}) copy-start(bf16[2,4,8,256]{3,2,1,0:T(8,128)(2,1)} %param.23) | copy-start | bytes 98308
  1.9 28.7 %collective-permute-start = (bf16[96,4096]{1,0:T(8,128)(2,1)S(1)}, bf16[96,4096]{1,0:T(8,128)(2,1)S(1)}, u32[]{:S(2)}, u32[]{:S(2)}) collective-permute-start(bf16[96,4096]{1,0:T(8,128)(2,1)S(1)} %pad_maximum_fusion.w_own), channel_id=1, source_target_pairs={{0,2},{2,0},{4,6},{6,4},{8,10},{10,8},{12,14},{14,12},{1,15},{3,5}... | collective-permute-start | bytes 2359304 | tf_op jit(solution)/shard_map/ppermute | solution.py:233
  7.8 30.1 %collective-permute-start.1 = (bf16[96,4096]{1,0:T(8,128)(2,1)S(1)}, bf16[96,4096]{1,0:T(8,128)(2,1)S(1)}, u32[]{:S(2)}, u32[]{:S(2)}) collective-permute-start(bf16[96,4096]{1,0:T(8,128)(2,1)S(1)} %pad_maximum_fusion.w_own), channel_id=1, source_target_pairs={{0,1},{1,0},{2,3},{3,2},{4,5},{5,4},{6,7},{7,6},{8,9},{9,8},{10,11... | collective-permute-start | bytes 2359304 | tf_op jit(solution)/shard_map/ppermute | solution.py:23
  13.9 39.9 %all-to-all-start = ((bf16[64,64,128]{2,1,0:T(8,128)(2,1)}), bf16[64,64,128]{2,1,0:T(8,128)(2,1)S(1)}, u32[]{:S(2)}, u32[]{:S(2)}) async-start(bf16[64,64,128]{2,1,0:T(8,128)(2,1)} %bitcast.66), calls=%async_computation | async-start | bytes 2097152 | tf_op jit(solution)/shard_map/all_to_all | solution.py:27
  27.2 5.6 %copy-start.11 = (f32[8]{0:T(128)}, f32[8]{0:T(128)S(1)}, u32[]{:S(2)}) copy-start(f32[8]{0:T(128)S(1)} %neg.17) | copy-start | bytes 100
  30.6 7.3 %copy-start.1 = (bf16[96,4096]{1,0:T(8,128)(2,1)}, bf16[96,4096]{1,0:T(8,128)(2,1)S(1)}, u32[]{:S(2)}) copy-start(bf16[96,4096]{1,0:T(8,128)(2,1)S(1)} %collective-permute-done.w_near) | copy-start | bytes 2359300
  30.6 8.2 %collective-permute-start.2 = (bf16[96,4096]{1,0:T(8,128)(2,1)S(1)}, bf16[96,4096]{1,0:T(8,128)(2,1)}, u32[]{:S(2)}, u32[]{:S(2)}) collective-permute-start(bf16[96,4096]{1,0:T(8,128)(2,1)S(1)} %collective-permute-done.w_near), channel_id=1, source_target_pairs={{0,1},{1,0},{2,3},{3,2},{4,5},{5,4},{6,7},{7,6},{8,9},{9,8},{10,11... | collective-permute-start | bytes 2359304 | tf_op jit(solution)/shard_map/ppermute | solution.py:23
  33.8 5.0 %copy-start.6 = (bf16[4096]{0:T(1024)(128)(2,1)S(1)}, bf16[4096]{0:T(1024)(128)(2,1)}, u32[]{:S(2)}) copy-start(bf16[4096]{0:T(1024)(128)(2,1)} %param.14) | copy-start | bytes 24580
  37.9 0.9 copy-start.3
  38.8 1.1 copy-start.2
  39.9 1.1 copy-start.4
  53.8 13.7 %copy-start.13 = (pred[2]{0:T(512)(128)(4,1)S(1)}, pred[2]{0:T(512)(128)(4,1)}, u32[]{:S(2)}) copy-start(pred[2]{0:T(512)(128)(4,1)} %iota_compare_fusion.2) | copy-start | bytes 10
  53.8 13.8 %copy-start.16 = (pred[192]{0:T(512)(128)(4,1)S(1)}, pred[192]{0:T(512)(128)(4,1)}, u32[]{:S(2)}) copy-start(pred[192]{0:T(512)(128)(4,1)} %fusion.15) | copy-start | bytes 580
  57.4 24.4 %copy-start.12 = (f32[4,8]{1,0:T(4,128)S(1)}, f32[4,8]{1,0:T(4,128)}, u32[]{:S(2)}) copy-start(f32[4,8]{1,0:T(4,128)} %multiply_exponential_fusion) | copy-start | bytes 388
  57.5 24.8 %copy-start.7 = (f32[2,8,128,256]{3,2,1,0:T(8,128)S(1)}, f32[2,8,128,256]{3,2,1,0:T(8,128)}, u32[]{:S(2)}) copy-start(f32[2,8,128,256]{3,2,1,0:T(8,128)} %multiply_add_fusion) | copy-start | bytes 6291460
  57.5 22.8 %all-to-all-start.1 = ((bf16[128,2,192]{2,1,0:T(2,128)(2,1)}), bf16[128,2,192]{2,1,0:T(2,128)(2,1)S(1)}, u32[]{:S(2)}, u32[]{:S(2)}) async-start(bf16[128,2,192]{2,1,0:T(2,128)(2,1)} %bitcast.11), calls=%async_computation.1 | async-start | bytes 262144 | tf_op jit(solution)/shard_map/all_to_all | solution.py:27
  81.8 2.3 %copy-start.9 = (bf16[2,4,8,128]{3,2,1,0:T(8,128)(2,1)}, bf16[2,4,8,128]{3,2,1,0:T(8,128)(2,1)S(1)}, u32[]{:S(2)}) copy-start(bf16[2,4,8,128]{3,2,1,0:T(8,128)(2,1)S(1)} %fusion.6) | copy-start | bytes 49156
  82.3 5.4 %copy-start.5 = (bf16[2048,64]{0,1:T(8,128)(2,1)S(1)}, bf16[2048,64]{0,1:T(8,128)(2,1)}, u32[]{:S(2)}) copy-start(bf16[2048,64]{0,1:T(8,128)(2,1)} %param.19) | copy-start | bytes 786436
  84.1 18.7 %all-to-all-start.2 = ((bf16[16,8,2048]{2,1,0:T(8,128)(2,1)}), bf16[16,8,2048]{2,1,0:T(8,128)(2,1)S(1)}, u32[]{:S(2)}, u32[]{:S(2)}) async-start(bf16[16,8,2048]{2,1,0:T(8,128)(2,1)} %broadcast_in_dim.50), calls=%async_computation.2 | async-start | bytes 1048576 | tf_op jit(solution)/shard_map/all_to_all | solution.py:27
  87.7 11.0 %collective-permute-start.3 = (bf16[64,2048]{1,0:T(8,128)(2,1)S(1)}, bf16[64,2048]{1,0:T(8,128)(2,1)S(1)}, u32[]{:S(2)}, u32[]{:S(2)}) collective-permute-start(bf16[64,2048]{1,0:T(8,128)(2,1)S(1)} %bitcast.62), channel_id=1, source_target_pairs={{0,32},{32,64},{64,96},{96,0},{1,97},{33,1},{65,33},{97,65},{2,34}... | collective-permute-start | bytes 786440 | tf_op jit(solution)/shard_map/ppermute | solution.py:243
  90.5 19.6 %collective-permute-start.4 = (bf16[64,2048]{1,0:T(8,128)(2,1)S(1)}, bf16[64,2048]{1,0:T(8,128)(2,1)S(1)}, u32[]{:S(2)}, u32[]{:S(2)}) collective-permute-start(bf16[64,2048]{1,0:T(8,128)(2,1)S(1)} %bitcast.63), channel_id=1, source_target_pairs={{32,0},{64,32},{96,64},{0,96},{97,1},{1,33},{33,65},{65,97},{34,2}... | collective-permute-start | bytes 786440 | tf_op jit(solution)/shard_map/ppermute | solution.py:243
  98.7 13.0 %collective-permute-start.5 = (bf16[64,2048]{1,0:T(8,128)(2,1)S(1)}, bf16[64,2048]{1,0:T(8,128)(2,1)S(1)}, u32[]{:S(2)}, u32[]{:S(2)}) collective-permute-start(bf16[64,2048]{1,0:T(8,128)(2,1)S(1)} %collective-permute-done.3.refs_1_), channel_id=1, source_target_pairs={{0,32},{32,64},{64,96},{96,0},{1,97},{33,1},{65,33},{97,65},{2,34}... | collective-permute-start | bytes 786440 | tf_op jit(solution)/shard_map/ppermute | solution.py:243
  113.5 20.0 %all-to-all-start.3 = ((bf16[8,32,128]{2,1,0:T(8,128)(2,1)}), bf16[8,32,128]{2,1,0:T(8,128)(2,1)S(1)}, u32[]{:S(2)}, u32[]{:S(2)}) async-start(bf16[8,32,128]{2,1,0:T(8,128)(2,1)} %output.1), calls=%async_computation.3 | async-start | bytes 131072 | tf_op jit(solution)/shard_map/all_to_all | solution.py:27

commit v3 on v2

--- a/solution.py
+++ b/solution.py
@@ -60,17 +60,16 @@
 
 
 def retain(query_rot, key_rot, value_rows, taken_state, log_decay):
-    highest = lax.Precision.HIGHEST
     step_ids = jnp.arange(query_rot.shape[1], dtype=jnp.int32)
     scores = jnp.einsum(
-        "sthd,smhd->shtm", query_rot.astype(FLOAT), key_rot.astype(FLOAT), precision=highest
+        "sthd,smhd->shtm", query_rot, key_rot, preferred_element_type=FLOAT
     )
     offset = (step_ids[:, None] - step_ids[None, :]).astype(FLOAT)
     decay_grid = jnp.where(
         offset[None] >= 0.0, jnp.exp(log_decay[:, None, None] * jnp.maximum(offset, 0.0)[None]), 0.0
     )
     inner_sum = jnp.einsum(
-        "shtm,smhe->sthe", scores * decay_grid[None], value_rows.astype(FLOAT), precision=highest
+        "shtm,smhe->sthe", scores * decay_grid[None], value_rows.astype(FLOAT), precision=lax.Precision.HIGH
     )
     query_decay = jnp.exp(log_decay[None, :] * (step_ids[:, None].astype(FLOAT) + 1.0))
     cross_sum = jnp.einsum(

time: 135 us -> 135 us (level)
  no operation moved by 1% of the time
where the time goes in v3:
time: 135 us; the launch traced here: 134 us
  starting transfers between devices  60 us (44%)
  waiting for transfers between devices  43.2 us (32%)
  Pallas kernels  8.78 us (7%)
  other arithmetic  8.19 us (6%)
  local copies, waits for them, and re-layouts  7.97 us (6%)
  matrix products  5.12 us (4%)
    all_to_all x4, starting transfers between devices, scattered(): return lax.all_to_all(blocks, axes, 0, 0, tiled=True)  37.7 us
    all_to_all x4, waiting for transfers between devices, scattered(): return lax.all_to_all(blocks, axes, 0, 0, tiled=True)  29.5 us
    ppermute x3, waiting for transfers between devices, turned_by(): return lax.ppermute(value, ('far_z', 'tp'), pairs)  13.7 us
    ppermute x3, starting transfers between devices, turned_by(): return lax.ppermute(value, ('far_z', 'tp'), pairs)  9.42 us
    ppermute x2, starting transfers between devices, moved(): lax.ppermute(value, axis, [(i, target(i) % size) for i in range(size)])  6.95 us
    ppermute x1, starting transfers between devices, shards(): w_near = lax.ppermute(w_own, ('y', 'tp'), neighbours)  5.92 us
    unnamed x42, local copies, waits for them, and re-layouts  4.16 us
    dot_general x1, matrix products, next_state(): jnp.einsum('sphd,sphe->shde', weighted_keys, last_values.astype(FLOAT), p...  4.12 us
  transfers between devices with their start and end apart: 10, of which 7 were waited for; matrix products, arithmetic and copies ran while one was open for 9% of the time, Pallas kernels for 2%

profile of v3, /device:TPU:1, one launch (start us, length us, event | category | flops | bytes accessed | tf_op | source)
XLA Modules:
  0.0 134.4 jit_solution(4627450735247082551)
XLA Ops:
  0.7 1.2 pad_maximum_fusion.w_own
  1.9 5.9 %collective-permute-start = (bf16[96,4096]{1,0:T(8,128)(2,1)S(1)}, bf16[96,4096]{1,0:T(8,128)(2,1)S(1)}, u32[]{:S(2)}, u32[]{:S(2)}) collective-permute-start(bf16[96,4096]{1,0:T(8,128)(2,1)S(1)} %pad_maximum_fusion.w_own), channel_id=1, source_target_pairs={{0,2},{2,0},{4,6},{6,4},{8,10},{10,8},{12,14},{14,12},{1,15},{3,5}... | collective-permute-start | bytes 2359304 | tf_op jit(solution)/shard_map/ppermute | solution.py:232
  7.8 4.8 %collective-permute-start.1 = (bf16[96,4096]{1,0:T(8,128)(2,1)S(1)}, bf16[96,4096]{1,0:T(8,128)(2,1)S(1)}, u32[]{:S(2)}, u32[]{:S(2)}) collective-permute-start(bf16[96,4096]{1,0:T(8,128)(2,1)S(1)} %pad_maximum_fusion.w_own), channel_id=1, source_target_pairs={{0,1},{1,0},{2,3},{3,2},{4,5},{5,4},{6,7},{7,6},{8,9},{9,8},{10,11... | collective-permute-start | bytes 2359304 | tf_op jit(solution)/shard_map/ppermute | solution.py:23
  12.6 1.3 broadcast_in_dim.44
  13.9 11.6 %all-to-all-start = ((bf16[64,64,128]{2,1,0:T(8,128)(2,1)}), bf16[64,64,128]{2,1,0:T(8,128)(2,1)S(1)}, u32[]{:S(2)}, u32[]{:S(2)}) async-start(bf16[64,64,128]{2,1,0:T(8,128)(2,1)} %bitcast.66), calls=%async_computation | async-start | bytes 2097152 | tf_op jit(solution)/shard_map/all_to_all | solution.py:27
  25.5 0.5 iota_compare_fusion.2
  26.0 0.5 fusion.15
  26.6 0.6 multiply_power_fusion
  27.2 0.6 multiply_exponential_fusion.1
  27.9 0.7 multiply_exponential_fusion
  28.5 0.6 convert_compare_fusion
  29.1 0.6 convert_maximum_fusion
  29.8 0.7 multiply_cosine_fusion
  30.6 2.2 %collective-permute-start.2 = (bf16[96,4096]{1,0:T(8,128)(2,1)S(1)}, bf16[96,4096]{1,0:T(8,128)(2,1)}, u32[]{:S(2)}, u32[]{:S(2)}) collective-permute-start(bf16[96,4096]{1,0:T(8,128)(2,1)S(1)} %collective-permute-done.w_near), channel_id=1, source_target_pairs={{0,1},{1,0},{2,3},{3,2},{4,5},{5,4},{6,7},{7,6},{8,9},{9,8},{10,11... | collective-permute-start | bytes 2359304 | tf_op jit(solution)/shard_map/ppermute | solution.py:23
  32.9 0.8 exponential_select_fusion
  33.8 4.1 %multiply_add_fusion = f32[2,8,128,256]{3,2,1,0:T(8,128)} fusion(f32[2,8,128,256]{3,2,1,0:T(8,128)} %param.21, f32[2,8]{1,0:T(2,128)} %multiply_exponential_fusion.1, bf16[2,4,8,256]{3,2,1,0:T(8,128)(2,1)S(1)} %copy-done.8, f32[2,4,8,128]{3,2,1,0:T(8,128)S(1)} %convert_multiply_fusion.1), kind=kOutput, calls=%fused_computation | convolution fusion | flops 26214400 | bytes 4259904 | tf_op jit(solution)/shard_map/sphd,sphe->shde/dot_general | solution.py:57
  37.9 0.9 copy-done.3
  38.8 1.1 copy-done.2
  40.0 1.1 copy-done.4
  41.1 3.3 %arrange.1 = (bf16[384,4096]{1,0:T(8,128)(2,1)}, bf16[4096,128]{1,0:T(8,128)(2,1)S(1)}) custom-call(s32[2]{0:T(128)S(1)} %pad_add_fusion.1.place, bf16[32,128]{1,0:T(8,128)(2,1)S(1)} %bitcast.65, bf16[96,4096]{1,0:T(8,128)(2,1)S(1)} %pad_maximum_fusion.w_own, bf16[96,4096]{1,0:T(8,128)(2,1)S(1)} %copy-done.2, bf16[96,4096]{1,0:T(8,128)(2,1)S(1)} %copy-done.4, ...), custom_call_target="tpu_custom_call" | custom-call | tf_op jit(solution)/shard_map/arrange/pallas_call | solution.py:112
  44.3 9.4 %all-to-all-done = bf16[64,64,128]{2,1,0:T(8,128)(2,1)S(1)} async-done(((bf16[64,64,128]{2,1,0:T(8,128)(2,1)}), bf16[64,64,128]{2,1,0:T(8,128)(2,1)S(1)}, u32[]{:S(2)}, u32[]{:S(2)}) %all-to-all-start) | async-done | bytes 1048608 | tf_op jit(solution)/shard_map/all_to_all | solution.py:27
  53.8 3.6 %project.1 = bf16[64,2,2,192]{3,2,1,0:T(2,128)(2,1)} custom-call(bf16[4096,128]{1,0:T(8,128)(2,1)S(1)} %bitcast.60, bf16[4096,128]{1,0:T(8,128)(2,1)S(1)} %get-tuple-element.8.gain, bf16[384,4096]{1,0:T(8,128)(2,1)} %get-tuple-element.9.far_weights), custom_call_target="tpu_custom_call" | custom-call | tf_op jit(solution)/shard_map/project/pallas_call | solution.py:144
  57.5 10.1 %all-to-all-start.1 = ((bf16[128,2,192]{2,1,0:T(2,128)(2,1)}), bf16[128,2,192]{2,1,0:T(2,128)(2,1)S(1)}, u32[]{:S(2)}, u32[]{:S(2)}) async-start(bf16[128,2,192]{2,1,0:T(2,128)(2,1)} %bitcast.11), calls=%async_computation.1 | async-start | bytes 262144 | tf_op jit(solution)/shard_map/all_to_all | solution.py:27
  67.6 12.6 %all-to-all-done.1 = bf16[128,2,192]{2,1,0:T(2,128)(2,1)S(1)} async-done(((bf16[128,2,192]{2,1,0:T(2,128)(2,1)}), bf16[128,2,192]{2,1,0:T(2,128)(2,1)S(1)}, u32[]{:S(2)}, u32[]{:S(2)}) %all-to-all-start.1) | async-done | bytes 98336 | tf_op jit(solution)/shard_map/all_to_all | solution.py:27
  80.2 0.1 fusion.16
  80.7 0.4 fusion.1
  81.2 0.1 reshape.323
  81.4 0.1 reshape.324
  81.5 0.1 reshape.316
  81.9 0.1 convolution_multiply_fusion
  82.1 0.2 fusion.20
  82.3 0.7 multiply_reduce_fusion
  83.0 0.1 reshape.319
  83.2 0.8 broadcast_in_dim.50
  84.0 3.6 %all-to-all-start.2 = ((bf16[16,8,2048]{2,1,0:T(8,128)(2,1)}), bf16[16,8,2048]{2,1,0:T(8,128)(2,1)S(1)}, u32[]{:S(2)}, u32[]{:S(2)}) async-start(bf16[16,8,2048]{2,1,0:T(8,128)(2,1)} %broadcast_in_dim.50), calls=%async_computation.2 | async-start | bytes 1048576 | tf_op jit(solution)/shard_map/all_to_all | solution.py:27
  87.6 2.9 %collective-permute-start.3 = (bf16[64,2048]{1,0:T(8,128)(2,1)S(1)}, bf16[64,2048]{1,0:T(8,128)(2,1)S(1)}, u32[]{:S(2)}, u32[]{:S(2)}) collective-permute-start(bf16[64,2048]{1,0:T(8,128)(2,1)S(1)} %bitcast.62), channel_id=1, source_target_pairs={{0,32},{32,64},{64,96},{96,0},{1,97},{33,1},{65,33},{97,65},{2,34}... | collective-permute-start | bytes 786440 | tf_op jit(solution)/shard_map/ppermute | solution.py:242
  90.5 3.3 %collective-permute-start.4 = (bf16[64,2048]{1,0:T(8,128)(2,1)S(1)}, bf16[64,2048]{1,0:T(8,128)(2,1)S(1)}, u32[]{:S(2)}, u32[]{:S(2)}) collective-permute-start(bf16[64,2048]{1,0:T(8,128)(2,1)S(1)} %bitcast.63), channel_id=1, source_target_pairs={{32,0},{64,32},{96,64},{0,96},{97,1},{1,33},{33,65},{65,97},{34,2}... | collective-permute-start | bytes 786440 | tf_op jit(solution)/shard_map/ppermute | solution.py:242
  93.8 4.8 %collective-permute-done.3.refs_1_ = bf16[64,2048]{1,0:T(8,128)(2,1)S(1)} collective-permute-done((bf16[64,2048]{1,0:T(8,128)(2,1)S(1)}, bf16[64,2048]{1,0:T(8,128)(2,1)S(1)}, u32[]{:S(2)}, u32[]{:S(2)}) %collective-permute-start.3) | collective-permute-done | bytes 262176 | tf_op jit(solution)/shard_map/ppermute | solution.py:242
  98.7 3.2 %collective-permute-start.5 = (bf16[64,2048]{1,0:T(8,128)(2,1)S(1)}, bf16[64,2048]{1,0:T(8,128)(2,1)S(1)}, u32[]{:S(2)}, u32[]{:S(2)}) collective-permute-start(bf16[64,2048]{1,0:T(8,128)(2,1)S(1)} %collective-permute-done.3.refs_1_), channel_id=1, source_target_pairs={{0,32},{32,64},{64,96},{96,0},{1,97},{33,1},{65,33},{97,65},{2,34}... | collective-permute-start | bytes 786440 | tf_op jit(solution)/shard_map/ppermute | solution.py:242
  102.0 0.8 all-to-all-done.2
  102.8 7.3 %collective-permute-done.4.refs_2_ = bf16[64,2048]{1,0:T(8,128)(2,1)S(1)} collective-permute-done((bf16[64,2048]{1,0:T(8,128)(2,1)S(1)}, bf16[64,2048]{1,0:T(8,128)(2,1)S(1)}, u32[]{:S(2)}, u32[]{:S(2)}) %collective-permute-start.4) | collective-permute-done | bytes 262176 | tf_op jit(solution)/shard_map/ppermute | solution.py:242
  110.1 1.5 %collective-permute-done.5.refs_3_ = bf16[64,2048]{1,0:T(8,128)(2,1)S(1)} collective-permute-done((bf16[64,2048]{1,0:T(8,128)(2,1)S(1)}, bf16[64,2048]{1,0:T(8,128)(2,1)S(1)}, u32[]{:S(2)}, u32[]{:S(2)}) %collective-permute-start.5) | collective-permute-done | bytes 262176 | tf_op jit(solution)/shard_map/ppermute | solution.py:242
  111.6 1.9 %output.1 = bf16[8,32,128]{2,1,0:T(8,128)(2,1)} custom-call(s32[2]{0:T(128)S(1)} %pad_add_fusion.place, bf16[128,2048]{1,0:T(8,128)(2,1)S(1)} %bitcast.61, bf16[64,2048]{1,0:T(8,128)(2,1)S(1)} %bitcast.64, bf16[64,2048]{1,0:T(8,128)(2,1)S(1)} %collective-permute-done.3.refs_1_, bf16[64,2048]{1,0:T(8,128)(2,1)S(1)} %collective-permute-done.4.refs_2_, ...), custom_call_target="tpu_custom_call" | custom-call | tf_op jit(solution)/shard_map/output/pallas_call | solution.py:185
  113.5 12.5 %all-to-all-start.3 = ((bf16[8,32,128]{2,1,0:T(8,128)(2,1)}), bf16[8,32,128]{2,1,0:T(8,128)(2,1)S(1)}, u32[]{:S(2)}, u32[]{:S(2)}) async-start(bf16[8,32,128]{2,1,0:T(8,128)(2,1)} %output.1), calls=%async_computation.3 | async-start | bytes 131072 | tf_op jit(solution)/shard_map/all_to_all | solution.py:27
  126.1 0.1 reshape.325
  126.2 0.6 copy.48
  126.8 6.7 %all-to-all-done.3 = bf16[8,32,128]{2,1,0:T(8,128)(2,1)S(1)} async-done(((bf16[8,32,128]{2,1,0:T(8,128)(2,1)}), bf16[8,32,128]{2,1,0:T(8,128)(2,1)S(1)}, u32[]{:S(2)}, u32[]{:S(2)}) %all-to-all-start.3) | async-done | bytes 65568 | tf_op jit(solution)/shard_map/all_to_all | solution.py:27
  133.7 0.7 copy.43
  (66 shorter events, 1.7 us)
Async XLA Ops:
  0.6 12.0 %copy-start = (bf16[128,4,64]{0,2,1:T(8,128)(2,1)S(1)}, bf16[128,4,64]{0,2,1:T(8,128)(2,1)}, u32[]{:S(2)}) copy-start(bf16[128,4,64]{0,2,1:T(8,128)(2,1)} %param.13) | copy-start | bytes 196612
  0.6 26.5 %copy-start.14 = (s32[2]{0:T(128)S(1)}, s32[2]{0:T(128)}, u32[]{:S(2)}) copy-start(s32[2]{0:T(128)} %param.24) | copy-start | bytes 28
  0.7 26.5 %copy-start.15 = (s32[2]{0:T(128)S(1)}, s32[2]{0:T(128)}, u32[]{:S(2)}) copy-start(s32[2]{0:T(128)} %param.25) | copy-start | bytes 28
  0.7 26.5 %copy-start.17 = (f32[8]{0:T(128)S(1)}, f32[8]{0:T(128)}, u32[]{:S(2)}) copy-start(f32[8]{0:T(128)} %param.20) | copy-start | bytes 100
  0.7 33.0 %copy-start.10 = (bf16[2,4,8,128]{3,2,1,0:T(8,128)(2,1)S(1)}, bf16[2,4,8,128]{3,2,1,0:T(8,128)(2,1)}, u32[]{:S(2)}) copy-start(bf16[2,4,8,128]{3,2,1,0:T(8,128)(2,1)} %param.22) | copy-start | bytes 49156
  0.7 33.1 %copy-start.8 = (bf16[2,4,8,256]{3,2,1,0:T(8,128)(2,1)S(1)}, bf16[2,4,8,256]{3,2,1,0:T(8,128)(2,1)}, u32[]{:S(2)}) copy-start(bf16[2,4,8,256]{3,2,1,0:T(8,128)(2,1)} %param.23) | copy-start | bytes 98308
  1.9 28.7 %collective-permute-start = (bf16[96,4096]{1,0:T(8,128)(2,1)S(1)}, bf16[96,4096]{1,0:T(8,128)(2,1)S(1)}, u32[]{:S(2)}, u32[]{:S(2)}) collective-permute-start(bf16[96,4096]{1,0:T(8,128)(2,1)S(1)} %pad_maximum_fusion.w_own), channel_id=1, source_target_pairs={{0,2},{2,0},{4,6},{6,4},{8,10},{10,8},{12,14},{14,12},{1,15},{3,5}... | collective-permute-start | bytes 2359304 | tf_op jit(solution)/shard_map/ppermute | solution.py:232
  7.8 30.1 %collective-permute-start.1 = (bf16[96,4096]{1,0:T(8,128)(2,1)S(1)}, bf16[96,4096]{1,0:T(8,128)(2,1)S(1)}, u32[]{:S(2)}, u32[]{:S(2)}) collective-permute-start(bf16[96,4096]{1,0:T(8,128)(2,1)S(1)} %pad_maximum_fusion.w_own), channel_id=1, source_target_pairs={{0,1},{1,0},{2,3},{3,2},{4,5},{5,4},{6,7},{7,6},{8,9},{9,8},{10,11... | collective-permute-start | bytes 2359304 | tf_op jit(solution)/shard_map/ppermute | solution.py:23
  13.9 39.9 %all-to-all-start = ((bf16[64,64,128]{2,1,0:T(8,128)(2,1)}), bf16[64,64,128]{2,1,0:T(8,128)(2,1)S(1)}, u32[]{:S(2)}, u32[]{:S(2)}) async-start(bf16[64,64,128]{2,1,0:T(8,128)(2,1)} %bitcast.66), calls=%async_computation | async-start | bytes 2097152 | tf_op jit(solution)/shard_map/all_to_all | solution.py:27
  27.2 5.6 %copy-start.11 = (f32[8]{0:T(128)}, f32[8]{0:T(128)S(1)}, u32[]{:S(2)}) copy-start(f32[8]{0:T(128)S(1)} %neg.17) | copy-start | bytes 100
  30.6 7.3 %copy-start.1 = (bf16[96,4096]{1,0:T(8,128)(2,1)}, bf16[96,4096]{1,0:T(8,128)(2,1)S(1)}, u32[]{:S(2)}) copy-start(bf16[96,4096]{1,0:T(8,128)(2,1)S(1)} %collective-permute-done.w_near) | copy-start | bytes 2359300
  30.6 8.2 %collective-permute-start.2 = (bf16[96,4096]{1,0:T(8,128)(2,1)S(1)}, bf16[96,4096]{1,0:T(8,128)(2,1)}, u32[]{:S(2)}, u32[]{:S(2)}) collective-permute-start(bf16[96,4096]{1,0:T(8,128)(2,1)S(1)} %collective-permute-done.w_near), channel_id=1, source_target_pairs={{0,1},{1,0},{2,3},{3,2},{4,5},{5,4},{6,7},{7,6},{8,9},{9,8},{10,11... | collective-permute-start | bytes 2359304 | tf_op jit(solution)/shard_map/ppermute | solution.py:23
  33.8 5.0 %copy-start.6 = (bf16[4096]{0:T(1024)(128)(2,1)S(1)}, bf16[4096]{0:T(1024)(128)(2,1)}, u32[]{:S(2)}) copy-start(bf16[4096]{0:T(1024)(128)(2,1)} %param.14) | copy-start | bytes 24580
  37.9 0.9 copy-start.3
  38.8 1.1 copy-start.2
  39.9 1.1 copy-start.4
  53.8 13.7 %copy-start.13 = (pred[2]{0:T(512)(128)(4,1)S(1)}, pred[2]{0:T(512)(128)(4,1)}, u32[]{:S(2)}) copy-start(pred[2]{0:T(512)(128)(4,1)} %iota_compare_fusion.2) | copy-start | bytes 10
  53.8 13.8 %copy-start.16 = (pred[192]{0:T(512)(128)(4,1)S(1)}, pred[192]{0:T(512)(128)(4,1)}, u32[]{:S(2)}) copy-start(pred[192]{0:T(512)(128)(4,1)} %fusion.15) | copy-start | bytes 580
  57.4 24.4 %copy-start.12 = (f32[4,8]{1,0:T(4,128)S(1)}, f32[4,8]{1,0:T(4,128)}, u32[]{:S(2)}) copy-start(f32[4,8]{1,0:T(4,128)} %multiply_exponential_fusion) | copy-start | bytes 388
  57.5 24.8 %copy-start.7 = (f32[2,8,128,256]{3,2,1,0:T(8,128)S(1)}, f32[2,8,128,256]{3,2,1,0:T(8,128)}, u32[]{:S(2)}) copy-start(f32[2,8,128,256]{3,2,1,0:T(8,128)} %multiply_add_fusion) | copy-start | bytes 6291460
  57.5 22.8 %all-to-all-start.1 = ((bf16[128,2,192]{2,1,0:T(2,128)(2,1)}), bf16[128,2,192]{2,1,0:T(2,128)(2,1)S(1)}, u32[]{:S(2)}, u32[]{:S(2)}) async-start(bf16[128,2,192]{2,1,0:T(2,128)(2,1)} %bitcast.11), calls=%async_computation.1 | async-start | bytes 262144 | tf_op jit(solution)/shard_map/all_to_all | solution.py:27
  81.8 2.2 %copy-start.9 = (bf16[2,4,8,128]{3,2,1,0:T(8,128)(2,1)}, bf16[2,4,8,128]{3,2,1,0:T(8,128)(2,1)S(1)}, u32[]{:S(2)}) copy-start(bf16[2,4,8,128]{3,2,1,0:T(8,128)(2,1)S(1)} %fusion.6) | copy-start | bytes 49156
  82.2 5.4 %copy-start.5 = (bf16[2048,64]{0,1:T(8,128)(2,1)S(1)}, bf16[2048,64]{0,1:T(8,128)(2,1)}, u32[]{:S(2)}) copy-start(bf16[2048,64]{0,1:T(8,128)(2,1)} %param.19) | copy-start | bytes 786436
  84.0 18.7 %all-to-all-start.2 = ((bf16[16,8,2048]{2,1,0:T(8,128)(2,1)}), bf16[16,8,2048]{2,1,0:T(8,128)(2,1)S(1)}, u32[]{:S(2)}, u32[]{:S(2)}) async-start(bf16[16,8,2048]{2,1,0:T(8,128)(2,1)} %broadcast_in_dim.50), calls=%async_computation.2 | async-start | bytes 1048576 | tf_op jit(solution)/shard_map/all_to_all | solution.py:27
  87.6 11.0 %collective-permute-start.3 = (bf16[64,2048]{1,0:T(8,128)(2,1)S(1)}, bf16[64,2048]{1,0:T(8,128)(2,1)S(1)}, u32[]{:S(2)}, u32[]{:S(2)}) collective-permute-start(bf16[64,2048]{1,0:T(8,128)(2,1)S(1)} %bitcast.62), channel_id=1, source_target_pairs={{0,32},{32,64},{64,96},{96,0},{1,97},{33,1},{65,33},{97,65},{2,34}... | collective-permute-start | bytes 786440 | tf_op jit(solution)/shard_map/ppermute | solution.py:242
  90.5 19.6 %collective-permute-start.4 = (bf16[64,2048]{1,0:T(8,128)(2,1)S(1)}, bf16[64,2048]{1,0:T(8,128)(2,1)S(1)}, u32[]{:S(2)}, u32[]{:S(2)}) collective-permute-start(bf16[64,2048]{1,0:T(8,128)(2,1)S(1)} %bitcast.63), channel_id=1, source_target_pairs={{32,0},{64,32},{96,64},{0,96},{97,1},{1,33},{33,65},{65,97},{34,2}... | collective-permute-start | bytes 786440 | tf_op jit(solution)/shard_map/ppermute | solution.py:242
  98.7 13.0 %collective-permute-start.5 = (bf16[64,2048]{1,0:T(8,128)(2,1)S(1)}, bf16[64,2048]{1,0:T(8,128)(2,1)S(1)}, u32[]{:S(2)}, u32[]{:S(2)}) collective-permute-start(bf16[64,2048]{1,0:T(8,128)(2,1)S(1)} %collective-permute-done.3.refs_1_), channel_id=1, source_target_pairs={{0,32},{32,64},{64,96},{96,0},{1,97},{33,1},{65,33},{97,65},{2,34}... | collective-permute-start | bytes 786440 | tf_op jit(solution)/shard_map/ppermute | solution.py:242
  113.5 20.0 %all-to-all-start.3 = ((bf16[8,32,128]{2,1,0:T(8,128)(2,1)}), bf16[8,32,128]{2,1,0:T(8,128)(2,1)S(1)}, u32[]{:S(2)}, u32[]{:S(2)}) async-start(bf16[8,32,128]{2,1,0:T(8,128)(2,1)} %output.1), calls=%async_computation.3 | async-start | bytes 131072 | tf_op jit(solution)/shard_map/all_to_all | solution.py:27
